TPU v7x, 512 devices: a whole 4x4x16 slice. The times are simulated.
512 devices in a mesh: dp: 4 (over x), kv: 64 (over z, y), tp: 2 (over core).
Axes of the slice: x: 4, y: 4, z: 16, core: 2. Of those that a mesh axis runs over, the one named last changes fastest.
Arguments:
- tokens: bfloat16 [2048, 4096], P('dp', ('kv', 'tp')), parts along dimension 0, may hold values from -12 to 12
- norm_gain: float32 [4096], replicated, may hold values from 0.1 to 1.9
- w_query: bfloat16 [4096, 3072], P(None, ('kv', 'tp')), may hold values from -0.09375 to 0.09375
- w_key: bfloat16 [4096, 3072], P(None, ('kv', 'tp')), may hold values from -0.09375 to 0.09375
- w_value: bfloat16 [4096, 3072], P(None, ('kv', 'tp')), may hold values from -0.09375 to 0.09375
- w_gate: bfloat16 [4096, 3072], P(None, ('kv', 'tp')), may hold values from -0.09375 to 0.09375
- w_output: bfloat16 [3072, 4096], P(None, ('kv', 'tp')), may hold values from -0.109375 to 0.109375
- decay_rate: float32 [24], replicated, may hold values from 0.003 to 2
- state: float32 [512, 24, 128, 128], P(('dp', 'kv', 'tp')), parts along dimension 0, may hold values from -0.54 to 0.54
- prev_keys: bfloat16 [512, 4, 3072], P(('dp', 'kv', 'tp')), parts along dimension 0, may hold values from -0.5390625 to 0.5390625
- prev_values: bfloat16 [512, 4, 3072], P(('dp', 'kv', 'tp')), parts along dimension 0, may hold values from -6 to 6
- accepted: int32 [512], P(('dp', 'kv', 'tp')), parts along dimension 0, may hold values from 0 to 4
- parents: int32 [512, 4], P(('dp', 'kv', 'tp')), parts along dimension 0, may hold values from -1 to 2, as said below
- seq_length: int32 [512], P(('dp', 'kv', 'tp')), parts along dimension 0, may hold values from 1 to 8191
Outputs:
- output: bfloat16 [2048, 4096], P('dp', ('kv', 'tp')), parts along dimension 0
- carried: float32 [512, 24, 128, 128], P(('dp', 'kv', 'tp')), parts along dimension 0
There are 4 independent parts, one for each index of `dp`. A program takes and returns all parts, laid end to end along the dimension named above; an argument that names none is the same for every part. Nothing has to cross between parts.
Inputs may be any that keep to these rules, and one draw needn't show every extreme that they name: parents[s, i] is -1 or an earlier proposal of the same sequence; proposal 0 has -1.
All inputs are finite; a program needn't handle non-finite values.
Results may differ from a plain program's by a relative error of at most 0.013.
Values may be sent and summed in bfloat16 or wider, within the bound.
A program may use at most 64 MiB of HBM per device.

v0:
```python
import jax
import jax.numpy as jnp
from jax import lax
from jax.sharding import Mesh
from jax.sharding import PartitionSpec as P

KV_TP = ("kv_0", "kv_1", "tp")
DP_KV_TP = ("dp", "kv_0", "kv_1", "tp")


EPS = 1e-06
HIGH = lax.Precision.HIGHEST


def from_everyone(array, axis):
    copies = jnp.broadcast_to(array, (lax.axis_size(axis), *array.shape))
    return lax.all_to_all(copies, axis, split_axis=0, concat_axis=0, tiled=True)


def in_order(pieces, dim):
    pieces = jnp.moveaxis(pieces, 0, dim)
    dims = pieces.shape
    return pieces.reshape(*dims[:dim], dims[dim] * dims[dim + 1], *dims[dim + 2 :])


def whole_of(array, axes, dim):
    far, near = axes
    initial = from_everyone(array, far)
    pieces = jnp.swapaxes(from_everyone(initial, near), 0, 1)
    return in_order(pieces.reshape(-1, *array.shape), dim)


def rotate(tensor, positions):
    half_dim = tensor.shape[-1] // 2
    frequency = 10000.0 ** (-jnp.arange(half_dim, dtype=jnp.float32) / half_dim)
    angles = positions[:, :, None] * frequency[None, None, :]
    cosine = jnp.cos(angles)[:, :, None, :]
    sine_part = jnp.sin(angles)[:, :, None, :]
    first = tensor[..., :half_dim]
    second = tensor[..., half_dim:]
    return jnp.concatenate(
        [first * cosine - second * sine_part, second * cosine + first * sine_part], axis=-1
    )


def ancestry_of(parents):
    props = parents.shape[1]
    linked = (parents[:, :, None] == jnp.arange(props, dtype=jnp.int32)[None, None, :]).astype(
        jnp.float32
    )
    identity = jnp.broadcast_to(jnp.eye(props, dtype=jnp.float32), linked.shape)
    ancestry = identity
    power = identity
    for hop in range(props - 1):
        power = jnp.einsum("bij,bjk->bik", power, linked, precision=HIGH)
        ancestry = ancestry + power
    depths = jnp.sum(ancestry, axis=-1) - 1.0
    return (ancestry, depths)


def advance(state, prev_keys, prev_values, accepted, decays):
    nseq, props, width = prev_keys.shape
    heads = decays.shape[0]
    head_dim = width // heads
    old_keys = prev_keys.astype(jnp.float32).reshape(nseq, props, heads, head_dim)
    old_values = prev_values.astype(jnp.float32).reshape(nseq, props, heads, head_dim)
    steps_done = accepted.astype(jnp.float32)[:, None]
    index = jnp.arange(props, dtype=jnp.float32)[None, :]
    age = jnp.maximum(steps_done - 1.0 - index, 0.0)
    weights = jnp.where(
        (index < steps_done)[:, :, None], jnp.exp(-decays[None, None, :] * age[:, :, None]), 0.0
    )
    kept = jnp.exp(-decays[None, :] * steps_done)
    added = jnp.einsum("bphd,bphe->bhde", old_keys * weights[..., None], old_values, precision=HIGH)
    return kept[:, :, None, None] * state + added


def retain(queries, key_rows, val_rows, gate_rows, decays, carried, parents, accepted, seq_length):
    nseq, props, heads, head_dim = queries.shape
    ancestry, depths = ancestry_of(parents)
    positions = (seq_length + accepted).astype(jnp.float32)[:, None] + depths
    rotated_q = rotate(queries.astype(jnp.float32), positions)
    rotated_k = rotate(key_rows.astype(jnp.float32), positions) * head_dim ** (-0.5)
    scores = jnp.einsum("bihd,bjhd->bhij", rotated_q, rotated_k, precision=HIGH)
    spacing = jnp.maximum(depths[:, :, None] - depths[:, None, :], 0.0)
    weighting = ancestry[:, None] * jnp.exp(-decays[None, :, None, None] * spacing[:, None])
    within = jnp.einsum(
        "bhij,bjhe->bihe", scores * weighting, val_rows.astype(jnp.float32), precision=HIGH
    )
    state_scale = jnp.exp(-decays[None, None, :] * (depths[:, :, None] + 1.0))
    from_state = (
        jnp.einsum("bihd,bhde->bihe", rotated_q, carried, precision=HIGH) * state_scale[..., None]
    )
    mixed_raw = within + from_state
    average = jnp.mean(mixed_raw, axis=-1, keepdims=True)
    centred = mixed_raw - average
    variance = jnp.mean(centred * centred, axis=-1, keepdims=True)
    normed = (centred * lax.rsqrt(variance + EPS)).reshape(nseq * props, heads * head_dim)
    gates = gate_rows.astype(jnp.float32).reshape(nseq * props, heads * head_dim)
    return (normed * jax.nn.silu(gates)).astype(jnp.bfloat16)


def per_device(
    tokens,
    norm_gain,
    w_query,
    w_key,
    w_value,
    w_gate,
    w_output,
    decay_rate,
    state,
    prev_keys,
    prev_values,
    accepted,
    parents,
    seq_length,
):
    weights = jnp.concatenate([w_query, w_key, w_value, w_gate], axis=1)
    columns = weights.shape[1]
    whole = whole_of(tokens, (("kv_0", "kv_1"), "tp"), 1).astype(jnp.float32)
    scale = lax.rsqrt(jnp.mean(whole * whole, axis=1, keepdims=True) + EPS)
    full_normed = (whole * scale * norm_gain[None, :]).astype(jnp.bfloat16)
    projected = jnp.dot(full_normed, weights, preferred_element_type=jnp.float32)
    rows_count = tokens.shape[0]
    projected = projected.astype(jnp.bfloat16).reshape(rows_count, 4, columns // 4)
    regrouped = lax.all_to_all(projected, KV_TP, split_axis=0, concat_axis=2, tiled=True)
    nseq = state.shape[0]
    heads = decay_rate.shape[0]
    head_dim = state.shape[2]
    props = parents.shape[1]

    def shaped(role):
        return regrouped[:, role].reshape(nseq, props, heads, head_dim)

    carried = advance(state, prev_keys, prev_values, accepted, decay_rate)
    mixed = retain(
        shaped(0),
        shaped(1),
        shaped(2),
        shaped(3),
        decay_rate,
        carried,
        parents,
        accepted,
        seq_length,
    )
    output = jnp.dot(
        whole_of(mixed, (("kv_0", "kv_1"), "tp"), 0), w_output, preferred_element_type=jnp.float32
    ).astype(jnp.bfloat16)
    return (output, carried)


def solution(mesh):
    torus = Mesh(
        mesh.devices.reshape(mesh.shape["dp"], 16, 4, mesh.shape["tp"]),
        ("dp", "kv_0", "kv_1", "tp"),
    )
    in_specs = (
        P("dp", KV_TP),
        P(),
        P(None, KV_TP),
        P(None, KV_TP),
        P(None, KV_TP),
        P(None, KV_TP),
        P(None, KV_TP),
        P(),
        P(DP_KV_TP, None, None, None),
        P(DP_KV_TP, None, None),
        P(DP_KV_TP, None, None),
        P(DP_KV_TP),
        P(DP_KV_TP, None),
        P(DP_KV_TP),
    )
    out_specs = (P("dp", KV_TP), P(DP_KV_TP, None, None, None))
    return jax.shard_map(
        per_device, mesh=torus, in_specs=in_specs, out_specs=out_specs, check_vma=False
    )
```

profile of v0, /device:TPU:1, one launch (start us, length us, event | category | flops | bytes accessed | tf_op | source)
XLA Modules:
  0.0 265.2 jit_solution(15990267746811270970)
XLA Ops:
  0.7 2.4 broadcast_in_dim.20
  3.0 19.3 %all-to-all-start = ((bf16[64,512,32]{1,2,0:T(8,128)(2,1)}), bf16[64,512,32]{1,2,0:T(8,128)(2,1)S(1)}, u32[]{:S(2)}, u32[]{:S(2)}) async-start(bf16[64,512,32]{1,2,0:T(8,128)(2,1)} %broadcast_in_dim.20), calls=%async_computation | async-start | bytes 4194304 | tf_op jit(solution)/shard_map/all_to_all | solution.py:17
  24.7 0.8 fusion.41
  26.3 91.0 %all-to-all-done = bf16[64,512,32]{1,2,0:T(8,128)(2,1)S(1)} async-done(((bf16[64,512,32]{1,2,0:T(8,128)(2,1)}), bf16[64,512,32]{1,2,0:T(8,128)(2,1)S(1)}, u32[]{:S(2)}, u32[]{:S(2)}) %all-to-all-start) | async-done | bytes 2097184 | tf_op jit(solution)/shard_map/all_to_all | solution.py:17
  117.3 0.7 broadcast_in_dim.21
  118.1 12.9 %all_to_all.38 = bf16[2,64,512,32]{2,3,1,0:T(8,128)(2,1)S(1)} all-to-all(bf16[2,64,512,32]{2,3,1,0:T(8,128)(2,1)S(1)} %broadcast_in_dim.21), channel_id=1, replica_groups=mesh['dp'=4,'kv_0'=16,'kv_1'=4,'tp'=2] {'tp'}, dimensions={0} | all-to-all | bytes 8388608 | tf_op jit(solution)/shard_map/all_to_all | solution.py:17
  131.0 1.0 multiply_reduce_fusion
  131.9 1.2 copy_convert_fusion
  133.2 1.5 fusion.1
  134.8 0.8 convolution_convert_fusion
  135.9 1.2 reshape.501
  137.1 6.5 %all-to-all-start.2 = ((bf16[128,2,192]{2,1,0:T(2,128)(2,1)}), bf16[128,2,192]{2,1,0:T(2,128)(2,1)S(1)}, u32[]{:S(2)}, u32[]{:S(2)}) async-start(bf16[128,2,192]{2,1,0:T(2,128)(2,1)} %reshape.501), calls=%async_computation.2 | async-start | bytes 262144 | tf_op jit(solution)/shard_map/all_to_all | solution.py:127
  143.6 0.6 subtract_maximum_fusion
  144.3 0.7 copy.38
  145.0 2.3 bitcast_add_fusion
  147.3 12.4 %all-to-all-done.2 = bf16[128,2,192]{2,1,0:T(2,128)(2,1)S(1)} async-done(((bf16[128,2,192]{2,1,0:T(2,128)(2,1)}), bf16[128,2,192]{2,1,0:T(2,128)(2,1)S(1)}, u32[]{:S(2)}, u32[]{:S(2)}) %all-to-all-start.2) | async-done | bytes 98336 | tf_op jit(solution)/shard_map/all_to_all | solution.py:127
  160.2 0.7 all_to_all.30
  161.3 1.5 fusion.8
  164.2 79.5 %all_to_all.39 = bf16[64,4,3072]{2,1,0:T(4,128)(2,1)S(1)} all-to-all(bf16[64,4,3072]{2,1,0:T(4,128)(2,1)S(1)} %broadcast_in_dim.24), channel_id=1, replica_groups=mesh['dp'=4,'kv_0'=16,'kv_1'=4,'tp'=2] {'kv_0','kv_1'}, dimensions={0} | all-to-all | bytes 3145728 | tf_op jit(solution)/shard_map/all_to_all | solution.py:17
  243.8 0.8 broadcast_in_dim.25
  244.6 11.0 %all_to_all.40 = bf16[2,64,4,3072]{3,2,1,0:T(4,128)(2,1)S(1)} all-to-all(bf16[2,64,4,3072]{3,2,1,0:T(4,128)(2,1)S(1)} %broadcast_in_dim.25), channel_id=1, replica_groups=mesh['dp'=4,'kv_0'=16,'kv_1'=4,'tp'=2] {'tp'}, dimensions={0} | all-to-all | bytes 6291456 | tf_op jit(solution)/shard_map/all_to_all | solution.py:17
  255.5 3.5 %copy.42 = bf16[64,2,4,3072]{3,2,1,0:T(4,128)(2,1)} copy(bf16[64,2,4,3072]{3,2,0,1:T(4,128)(2,1)S(1)} %bitcast.89) | data formatting | bytes 6291456 | tf_op jit(solution)/shard_map/transpose | solution.py:29
  259.1 4.5 %reshape_reshape.3 = bf16[512,3072]{1,0:T(8,128)(2,1)S(1)} reshape(bf16[64,2,4,3072]{3,2,1,0:T(4,128)(2,1)} %copy.42) | data formatting | bytes 6291456 | tf_op jit(solution)/shard_map/reshape;reshape | solution.py:23
  263.6 1.7 convolution_convert_fusion.1
  (60 shorter events, 4.6 us)
Async XLA Ops:
  0.6 262.9 %copy-start = (bf16[3072,32]{0,1:T(8,128)(2,1)S(1)}, bf16[3072,32]{0,1:T(8,128)(2,1)}, u32[]{:S(2)}) copy-start(bf16[3072,32]{0,1:T(8,128)(2,1)} %param.20) | copy-start | bytes 589828
  0.6 23.0 %copy-start.12 = (f32[24]{0:T(128)S(1)}, f32[24]{0:T(128)}, u32[]{:S(2)}) copy-start(f32[24]{0:T(128)} %param.21) | copy-start | bytes 292
  0.7 23.5 %copy-start.17 = (s32[1,4]{1,0:T(1,128)S(1)}, s32[1,4]{1,0:T(1,128)}, u32[]{:S(2)}) copy-start(s32[1,4]{1,0:T(1,128)} %param.26) | copy-start | bytes 52
  3.0 114.3 %all-to-all-start = ((bf16[64,512,32]{1,2,0:T(8,128)(2,1)}), bf16[64,512,32]{1,2,0:T(8,128)(2,1)S(1)}, u32[]{:S(2)}, u32[]{:S(2)}) async-start(bf16[64,512,32]{1,2,0:T(8,128)(2,1)} %broadcast_in_dim.20), calls=%async_computation | async-start | bytes 4194304 | tf_op jit(solution)/shard_map/all_to_all | solution.py:17
  24.2 93.8 %copy-start.10 = (f32[24]{0:T(128)}, f32[24]{0:T(128)S(1)}, u32[]{:S(2)}) copy-start(f32[24]{0:T(128)S(1)} %get-tuple-element.22) | copy-start | bytes 292
  131.9 1.2 copy-start.5
  133.1 1.5 copy-start.13
  133.2 1.5 copy-start.14
  133.2 1.5 copy-start.15
  133.2 1.5 copy-start.16
  134.7 8.9 %copy-start.6 = (f32[4]{0:T(128)S(1)}, f32[4]{0:T(128)}, u32[]{:S(2)}) copy-start(f32[4]{0:T(128)} %get-tuple-element.18) | copy-start | bytes 52
  134.7 9.6 %copy-start.9 = (f32[4,4]{0,1:T(4,128)S(1)}, f32[4,4]{0,1:T(4,128)}, u32[]{:S(2)}) copy-start(f32[4,4]{0,1:T(4,128)} %get-tuple-element.25) | copy-start | bytes 196
  134.7 10.2 %copy-start.2 = (f32[1,24,128,128]{3,2,1,0:T(8,128)S(1)}, f32[1,24,128,128]{3,2,1,0:T(8,128)}, u32[]{:S(2)}) copy-start(f32[1,24,128,128]{3,2,1,0:T(8,128)} %param.22) | copy-start | bytes 4718596
  134.7 10.2 %copy-start.3 = (bf16[1,4,3072]{2,1,0:T(4,128)(2,1)S(1)}, bf16[1,4,3072]{2,1,0:T(4,128)(2,1)}, u32[]{:S(2)}) copy-start(bf16[1,4,3072]{2,1,0:T(4,128)(2,1)} %param.23) | copy-start | bytes 73732
  134.7 10.2 %copy-start.4 = (bf16[1,4,3072]{2,1,0:T(4,128)(2,1)S(1)}, bf16[1,4,3072]{2,1,0:T(4,128)(2,1)}, u32[]{:S(2)}) copy-start(bf16[1,4,3072]{2,1,0:T(4,128)(2,1)} %param.24) | copy-start | bytes 73732
  137.1 22.6 %all-to-all-start.2 = ((bf16[128,2,192]{2,1,0:T(2,128)(2,1)}), bf16[128,2,192]{2,1,0:T(2,128)(2,1)S(1)}, u32[]{:S(2)}, u32[]{:S(2)}) async-start(bf16[128,2,192]{2,1,0:T(2,128)(2,1)} %reshape.501), calls=%async_computation.2 | async-start | bytes 262144 | tf_op jit(solution)/shard_map/all_to_all | solution.py:127
  147.2 15.6 %copy-start.1 = (f32[1,24,128,128]{3,2,1,0:T(8,128)}, f32[1,24,128,128]{3,2,1,0:T(8,128)S(1)}, u32[]{:S(2)}) copy-start(f32[1,24,128,128]{3,2,1,0:T(8,128)S(1)} %bitcast_add_fusion) | copy-start | bytes 4718596
  147.2 15.5 %copy-start.7 = (f32[4,4]{1,0:T(4,128)S(1)}, f32[4,4]{1,0:T(4,128)}, u32[]{:S(2)}) copy-start(f32[4,4]{1,0:T(4,128)} %subtract_maximum_fusion) | copy-start | bytes 196
  147.2 15.5 %copy-start.8 = (f32[4,4]{1,0:T(4,128)S(1)}, f32[4,4]{1,0:T(4,128)}, u32[]{:S(2)}) copy-start(f32[4,4]{1,0:T(4,128)} %copy.38) | copy-start | bytes 196
  147.3 15.5 %copy-start.11 = (f32[24]{0:T(128)S(1)}, f32[24]{0:T(128)}, u32[]{:S(2)}) copy-start(f32[24]{0:T(128)} %copy-done.10) | copy-start | bytes 292
where the time goes:
time: 266 us; the launch traced here: 265 us
  waiting for transfers between devices  103 us (39%)
  blocking collectives  103 us (39%)
  starting transfers between devices  25.8 us (10%)
  local copies, waits for them, and re-layouts  15.9 us (6%)
  matrix products  8.22 us (3%)
  other arithmetic  6.18 us (2%)
    all_to_all x3, blocking collectives, from_everyone(): return lax.all_to_all(copies, axis, split_axis=0, concat_axis=0, tiled=True)  103 us
    all_to_all x1, waiting for transfers between devices, from_everyone(): return lax.all_to_all(copies, axis, split_axis=0, concat_axis=0, tiled=True)  91 us
    all_to_all x1, starting transfers between devices, from_everyone(): return lax.all_to_all(copies, axis, split_axis=0, concat_axis=0, tiled=True)  19.3 us
    all_to_all x1, waiting for transfers between devices, per_device(): lax.all_to_all(projected, KV_TP, split_axis=0, concat_axis=2, tiled=True)  12.4 us
    all_to_all x1, starting transfers between devices, per_device(): lax.all_to_all(projected, KV_TP, split_axis=0, concat_axis=2, tiled=True)  6.54 us
  transfers between devices with their start and end apart: 2, of which 2 were waited for; matrix products, arithmetic and copies ran while one was open for 2% of the time, Pallas kernels for 0%

commit v1 on v0

v1 whole, which is shorter than its diff:
```python
import functools

import jax
import jax.numpy as jnp
from jax import lax
from jax.experimental import pallas as pl
from jax.experimental.pallas import tpu as pltpu
from jax.sharding import Mesh
from jax.sharding import PartitionSpec as P

KV_TP = ("kv_0", "kv_1", "tp")
DP_KV_TP = ("dp", "kv_0", "kv_1", "tp")
MESH = pl.DeviceIdType.MESH
EPS = 1e-06
F32 = jnp.float32
BF16 = jnp.bfloat16

NZ, NY = 16, 4
SLOTS = NZ * NY
HALF = NZ // 2


def iota(shape, axis):
    return lax.broadcasted_iota(jnp.int32, shape, axis)


def nt(a, b):
    return lax.dot_general(a, b, (((1,), (1,)), ((), ())), preferred_element_type=F32)


def tn(a, b):
    return lax.dot_general(a, b, (((0,), (0,)), ((), ())), preferred_element_type=F32)


def block_of(z, h, y):
    return z * (2 * NY) + h * NY + y


def sin_cos(angle):
    quarter = jnp.floor(angle * 0.6366197723675814 + 0.5)
    r = angle - quarter * 1.5703125
    r = r - quarter * 4.837512969970703125e-4
    r = r - quarter * 7.54978995489188216e-8
    r2 = r * r
    s = r + r * r2 * (-1.6666654611e-1 + r2 * (8.3321608736e-3 - r2 * 1.9515295891e-4))
    c = 1.0 - 0.5 * r2 + r2 * r2 * (
        4.166664568298827e-2 + r2 * (-1.388731625493765e-3 + r2 * 2.443315711809948e-5)
    )
    turn = quarter - 4.0 * jnp.floor(quarter * 0.25)
    swap = (turn == 1.0) | (turn == 3.0)
    sine = jnp.where(swap, c, s)
    cosine = jnp.where(swap, s, c)
    sine = jnp.where(turn >= 2.0, -sine, sine)
    cosine = jnp.where((turn == 1.0) | (turn == 2.0), -cosine, cosine)
    return sine, cosine


def gather_over_torus(buf, send_sem, recv_sem, place, between, compute):
    z, y = place
    z_up, z_down = lax.rem(z + 1, NZ), lax.rem(z + NZ - 1, NZ)
    y_up, y_down = lax.rem(y + 1, NY), lax.rem(y + NY - 1, NY)
    y_far = lax.rem(y + 2, NY)
    up, down = {"kv_0": z_up}, {"kv_0": z_down}
    right, left = {"kv_1": y_up}, {"kv_1": y_down}

    def copy(block, device):
        return pltpu.make_async_remote_copy(
            src_ref=buf.at[block],
            dst_ref=buf.at[block],
            send_sem=send_sem,
            recv_sem=recv_sem.at[block],
            device_id=device,
            device_id_type=MESH,
        )

    def send(block, device):
        copy(block, device).start()

    def arrive(block):
        copy(block, up).wait_recv()

    for h in (0, 1):
        own = block_of(z, h, y)
        send(own, up)
        send(own, down)
    for h in (0, 1):
        own = block_of(z, h, y)
        send(own, right)
        send(own, left)

    def along(k, h, ys, last_up, last_down, spread):
        z_from_down = lax.rem(z - k + 2 * NZ, NZ)
        z_from_up = lax.rem(z + k, NZ)

        @pl.when((k >= 1) & (k <= last_up))
        def _():
            block = block_of(z_from_down, h, ys)
            arrive(block)

            @pl.when(k < last_up)
            def _():
                send(block, up)

            if spread:
                send(block, right)
                send(block, left)

        @pl.when((k >= 1) & (k <= last_down))
        def _():
            block = block_of(z_from_up, h, ys)
            arrive(block)

            @pl.when(k < last_down)
            def _():
                send(block, down)

            if spread:
                send(block, right)
                send(block, left)

    def relay(zz, h, ys):
        block = block_of(zz, h, ys)
        even = lax.rem(zz, 2) == 0
        if ys is y_down:

            @pl.when(even)
            def _():
                send(block, right)

        elif ys is y_up:

            @pl.when(jnp.logical_not(even))
            def _():
                send(block, left)

    def across(k, ys):
        along(k, 0, ys, HALF, HALF - 1, False)

        @pl.when(k == 0)
        def _():
            block = block_of(z, 0, ys)
            arrive(block)
            send(block, up)
            send(block, down)
            relay(z, 0, ys)
            arrive(block_of(z, 1, ys))
            relay(z, 1, ys)

        @pl.when((k >= 1) & (k <= HALF - 1))
        def _():
            zz = lax.rem(z - k + 2 * NZ, NZ)
            arrive(block_of(zz, 1, ys))
            relay(zz, 1, ys)

        @pl.when((k >= 1) & (k <= HALF))
        def _():
            zz = lax.rem(z + k, NZ)
            arrive(block_of(zz, 1, ys))
            relay(zz, 1, ys)

    def step(t, carry):
        @pl.when(t <= HALF)
        def _():
            along(t, 0, y, HALF, HALF - 1, False)
            along(t, 1, y, HALF - 1, HALF, True)

        @pl.when(t <= HALF + 1)
        def _():
            across(t - 1, y_down)
            across(t - 1, y_up)

        @pl.when(t >= 2)
        def _():
            k = t - 2
            across(k, y_far)
            compute(lax.rem(z - k + 2 * NZ, NZ))

            @pl.when((k >= 1) & (k <= HALF - 1))
            def _():
                compute(lax.rem(z + k, NZ))

        between(t)
        return carry

    return step


def drain(buf, send_sem, recv_sem, count):
    pltpu.make_async_remote_copy(
        src_ref=buf.at[pl.ds(0, count)],
        dst_ref=buf.at[pl.ds(0, count)],
        send_sem=send_sem,
        recv_sem=recv_sem,
        device_id={"kv_0": lax.rem(lax.axis_index("kv_0") + 1, NZ)},
        device_id_type=MESH,
    ).wait_send()


def kernel(
    accepted_ref,
    parents_ref,
    length_ref,
    decay_ref,
    tok_hbm,
    gain_hbm,
    wq_hbm,
    wk_hbm,
    wv_hbm,
    wg_hbm,
    wo_hbm,
    state_hbm,
    pk_hbm,
    pv_hbm,
    out_ref,
    carried_hbm,
    tok,
    gain,
    w4,
    wo,
    state,
    pk,
    pv,
    order,
    tokens,
    weights,
    weights_out,
    acc,
    acc_in,
    rows,
    sent,
    got,
    table,
    carried_bf,
    decays,
    mixed,
    wo_in,
    w_cat,
    raw,
    final_out,
    final,
    load_sem,
    store_sem,
    pair_send,
    pair_recv,
    tok_send,
    tok_recv,
    a2a_send,
    a2a_recv,
    mix_send,
    mix_recv,
):
    z, y, c = lax.axis_index("kv_0"), lax.axis_index("kv_1"), lax.axis_index("tp")
    slot = z * NY + y
    other = {"tp": 1 - c}
    loads = [
        pltpu.make_async_copy(tok_hbm, tok, load_sem.at[0]),
        pltpu.make_async_copy(gain_hbm, gain, load_sem.at[1]),
        pltpu.make_async_copy(wq_hbm, w4.at[0], load_sem.at[2]),
        pltpu.make_async_copy(wk_hbm, w4.at[1], load_sem.at[3]),
        pltpu.make_async_copy(wv_hbm, w4.at[2], load_sem.at[4]),
        pltpu.make_async_copy(wg_hbm, w4.at[3], load_sem.at[5]),
        pltpu.make_async_copy(wo_hbm, wo, load_sem.at[6]),
        pltpu.make_async_copy(pk_hbm, pk, load_sem.at[7]),
        pltpu.make_async_copy(pv_hbm, pv, load_sem.at[8]),
        pltpu.make_async_copy(state_hbm, state, load_sem.at[9]),
    ]
    for load in loads:
        load.start()
    barrier = pltpu.get_barrier_semaphore()
    for device in (
        {"kv_0": lax.rem(z + 1, NZ)},
        {"kv_0": lax.rem(z + NZ - 1, NZ)},
        {"kv_1": lax.rem(y + 1, NY)},
        {"kv_1": lax.rem(y + NY - 1, NY)},
        other,
    ):
        pl.semaphore_signal(barrier, inc=1, device_id=device, device_id_type=MESH)

    t = iota((512, 512), 0)
    place = (lax.shift_right_logical(t, 2) & 1) * 256 + lax.shift_right_logical(t, 3) * 4 + (t & 3)
    order[...] = jnp.where(place == iota((512, 512), 1), 1.0, 0.0).astype(BF16)
    loads[0].wait()
    own = jnp.dot(tok[...], order[...], preferred_element_type=F32).astype(BF16)
    tokens[block_of(z, 0, y)] = own[:16]
    tokens[block_of(z, 1, y)] = own[16:]
    acc[...] = jnp.zeros_like(acc)
    pl.semaphore_wait(barrier, 5)

    def project(zz):
        x = tokens[pl.ds(zz * 8, 8)].reshape(128, 512)
        w = weights[:, :, pl.ds(pl.multiple_of(zz * 128, 128), 128)].reshape(192, 128)
        r = jnp.dot(w, x, preferred_element_type=F32)
        xf = x.astype(F32)
        squares = jnp.sum((xf * xf).reshape(16, 8, 512), axis=0)
        for half in (0, 1):
            lanes = slice(half * 256, half * 256 + 256)
            acc[half, :192] += r[:, lanes]
            acc[half, 192:] += squares[:, lanes]

    def advance(t):
        steps = accepted_ref[0].astype(F32)
        g = t - 1

        @pl.when(t == 1)
        def _():
            prepare_weights()
            for load in loads[6:]:
                load.wait()
            for h in range(24):
                decays[h] = jnp.broadcast_to(decay_ref[h], (8, 128))

        @pl.when((t >= 1) & (t <= 8))
        def _():
            lanes = pl.ds(pl.multiple_of(g * 384, 128), 384)
            keys = pk[:, lanes].astype(F32)
            values = pv[:, lanes]
            row = iota((4, 128), 0).astype(F32)
            for m in range(3):
                h = g * 3 + m
                r = decays[h]
                age = jnp.maximum(steps - 1.0 - row, 0.0)
                weight = jnp.where(row < steps, jnp.exp(-r[:4] * age), 0.0)
                part = slice(m * 128, m * 128 + 128)
                keyed = keys[:, part] * weight
                high = keyed.astype(BF16)
                low = (keyed - high.astype(F32)).astype(BF16)
                v = values[:, part]
                added = tn(high, v) + tn(low, v)
                kept = jnp.exp(-r[:1] * steps)
                new = state[h] * kept + added
                state[h] = new
                place = m * 8 + lax.rem(g, 2) * 4 + lax.div(g, 2)
                carried_bf[place] = new.astype(BF16)

        @pl.when(t == 9)
        def _():
            pltpu.make_async_copy(state, carried_hbm, store_sem).start()

    step = gather_over_torus(tokens, tok_send, tok_recv, (z, y), advance, project)
    weights_copy = pltpu.make_async_remote_copy(
        src_ref=weights_out,
        dst_ref=weights.at[c],
        send_sem=pair_send.at[0],
        recv_sem=pair_recv.at[0],
        device_id=other,
        device_id_type=MESH,
    )
    wo_copy = pltpu.make_async_remote_copy(
        src_ref=wo,
        dst_ref=wo_in,
        send_sem=pair_send.at[1],
        recv_sem=pair_recv.at[1],
        device_id=other,
        device_id_type=MESH,
    )

    def prepare_weights():
        f = iota((256, 256), 0)
        yy, cc = lax.shift_right_logical(f, 6), lax.shift_right_logical(f, 5) & 1
        hh, ii = lax.shift_right_logical(f, 4) & 1, f & 15
        split = jnp.where(cc * 128 + hh * 64 + yy * 16 + ii == iota((256, 256), 1), 1.0, 0.0)
        split = split.astype(BF16)
        for load in loads[1:6]:
            load.wait()

        def chunk(zz, carry):
            lanes = pl.ds(pl.multiple_of(zz * 256, 256), 256)
            scale = gain[:, lanes]
            w = jnp.concatenate([w4[r, :, lanes].astype(F32) * scale for r in range(4)], axis=0)
            w = jnp.dot(w.astype(BF16), split, preferred_element_type=F32).astype(BF16)
            half = pl.ds(pl.multiple_of(zz * 128, 128), 128)
            weights[c, :, half] = jnp.where(c == 0, w[:, :128], w[:, 128:])
            weights_out[:, half] = jnp.where(c == 0, w[:, 128:], w[:, :128])
            return carry

        lax.fori_loop(0, NZ, chunk, 0)
        weights_copy.start()
        weights_copy.wait_recv()

    lax.fori_loop(1, HALF + 3, step, 0)

    partial_copy = pltpu.make_async_remote_copy(
        src_ref=acc.at[1 - c],
        dst_ref=acc_in,
        send_sem=pair_send.at[2],
        recv_sem=pair_recv.at[2],
        device_id=other,
        device_id_type=MESH,
    )
    partial_copy.start()
    wo_copy.start()
    partial_copy.wait_recv()
    total = acc[c] + acc_in[...]
    mean = jnp.sum(total[192:], axis=0, keepdims=True) * (1.0 / 4096.0)
    total = total[:192] * lax.rsqrt(mean + EPS)
    pad = jnp.zeros((32, 256), F32)
    pieces = []
    for roles in ((0, 1), (2, 3)):
        for r in roles:
            pieces += [total[r * 24 : r * 24 + 24], total[96 + r * 24 : 96 + r * 24 + 24]]
        pieces.append(pad)
    by_token = jnp.concatenate(pieces, axis=0).T
    j = lax.rem(slot, 8)
    shift = lax.rem(j * 48, 128)
    rows[:, :128] = pltpu.roll(by_token[:, :128], shift, 1)
    rows[:, 128:] = pltpu.roll(by_token[:, 128:], shift, 1)

    def pack(i, carry):
        two = rows[pl.ds(pl.multiple_of(i * 8, 8), 8), :].astype(BF16)
        sent[2 * i] = two[:4]
        sent[2 * i + 1] = two[4:]
        return carry

    lax.fori_loop(0, SLOTS // 2, pack, 0)

    def dispatch(i, carry):
        target = lax.rem(slot + i, SLOTS)
        pltpu.make_async_remote_copy(
            src_ref=sent.at[target],
            dst_ref=got.at[slot],
            send_sem=a2a_send,
            recv_sem=a2a_recv,
            device_id={"kv_0": lax.div(target, NY), "kv_1": lax.rem(target, NY)},
            device_id_type=MESH,
        ).start()
        return carry

    lax.fori_loop(1, SLOTS, dispatch, 0)
    got[slot] = sent[slot]

    parent = [parents_ref[0, i] for i in range(4)]
    one, zero = jnp.float32(1.0), jnp.float32(0.0)
    anc = [[one if i == k else zero for k in range(4)] for i in range(4)]
    for i in range(1, 4):
        for k in range(i):
            value = zero
            for via in range(k, i):
                value = jnp.where(parent[i] == via, anc[via][k], value)
            anc[i][k] = value
    depth = [sum(anc[i][k] for k in range(i + 1)) - 1.0 for i in range(4)]

    def by_proposal(values, shape):
        p = iota(shape, 0) & 3
        result = jnp.broadcast_to(values[3], shape)
        for i in range(3):
            result = jnp.where(p == i, values[i], result)
        return result

    start = (length_ref[0] + accepted_ref[0]).astype(F32)
    lane = iota((8, 128), 1)
    freq = jnp.ones((8, 128), F32)
    for bit in range(6):
        freq = jnp.where((lane & (1 << bit)) != 0, freq * 10000.0 ** (-(2**bit) / 64.0), freq)
    sine, cosine = sin_cos(by_proposal([start + d for d in depth], (8, 128)) * freq)
    sine = jnp.where(lane < 64, -sine, sine)
    cosine = jnp.concatenate([cosine] * 4, axis=0)
    sine = jnp.concatenate([sine] * 4, axis=0)
    shape = (32, 128)
    depths = by_proposal(depth, shape)
    linked, spacing = [], []
    for d in range(4):
        linked.append(by_proposal([anc[i][i - d] if i >= d else zero for i in range(4)], shape))
        gap = [jnp.maximum(depth[i] - depth[i - d], 0.0) if i >= d else zero for i in range(4)]
        spacing.append(by_proposal(gap, shape))
    group = lax.shift_right_logical(iota(shape, 0), 2)
    near, carry_in = [], []
    for m in range(3):
        rate = jnp.zeros(shape, F32)
        for g in range(8):
            at = (g % 2) * 4 + g // 2
            rate = jnp.where(group == at, jnp.concatenate([decays[3 * g + m]] * 4, axis=0), rate)
        near.append([linked[d] * jnp.exp(-rate * spacing[d]) for d in range(4)])
        carry_in.append(jnp.exp(-rate * (depths + 1.0)))
    wo_copy.wait_recv()
    for b in range(2):
        for jj in range(4):
            lanes = slice((2 * jj + b) * 384, (2 * jj + b) * 384 + 384)
            mine, theirs = wo[:, lanes], wo_in[:, lanes]
            w_cat[b, jj * 64 : jj * 64 + 32] = jnp.where(c == 0, mine, theirs)
            w_cat[b, jj * 64 + 32 : jj * 64 + 64] = jnp.where(c == 0, theirs, mine)

    pltpu.make_async_remote_copy(
        src_ref=sent.at[pl.ds(0, SLOTS - 1)],
        dst_ref=got.at[pl.ds(0, SLOTS - 1)],
        send_sem=a2a_send,
        recv_sem=a2a_recv,
        device_id={"kv_0": lax.rem(z + 1, NZ)},
        device_id_type=MESH,
    ).wait()

    def unpack(jj, carry):
        for b in range(2):
            for q in range(4):
                g = 2 * q + b
                r = (b * 4 + q) * 4
                table[jj, r : r + 4, :] = got[g * 8 + jj].astype(F32)
        return carry

    lax.fori_loop(0, 8, unpack, 0)
    lane = iota(shape, 1)

    def heads(role):
        part = slice(0, 128) if role < 2 else slice(128, 256)
        held = [table[jj, :, part] for jj in range(8)]
        if role % 2:
            held = [pltpu.roll(x, 80, 1) for x in held]
        result = []
        for m in range(3):
            value = None
            for jj in range(8):
                low, high = max(48 * jj - 128 * m, 0), min(48 * jj + 48 - 128 * m, 128)
                if low < high:
                    value = held[jj] if value is None else jnp.where(lane >= low, held[jj], value)
            result.append(value)
        return result

    queries, keys, values, gates = heads(0), heads(1), heads(2), heads(3)
    for m in range(3):
        rq = queries[m] * cosine + pltpu.roll(queries[m], 64, 1) * sine
        rk = (keys[m] * cosine + pltpu.roll(keys[m], 64, 1) * sine) * (128.0**-0.5)
        rq16 = rq.astype(BF16)
        zeros = jnp.zeros_like(rq16)
        spread = jnp.concatenate([jnp.where(group == r, rq16, zeros) for r in range(8)], axis=1)
        held = carried_bf[m * 8 : m * 8 + 8].reshape(1024, 128)
        mixed_raw = jnp.dot(spread, held, preferred_element_type=F32) * carry_in[m]
        for d in range(4):
            rkd = rk if d == 0 else pltpu.roll(rk, d, 0)
            vd = values[m] if d == 0 else pltpu.roll(values[m], d, 0)
            mixed_raw += jnp.sum(rq * rkd, axis=1, keepdims=True) * near[m][d] * vd
        centred = mixed_raw - jnp.mean(mixed_raw, axis=1, keepdims=True)
        variance = jnp.mean(centred * centred, axis=1, keepdims=True)
        gate = gates[m]
        result = (centred * lax.rsqrt(variance + EPS)) * (gate / (1.0 + jnp.exp(-gate)))
        result = result.astype(BF16)
        for b in range(2):
            mixed[block_of(z, b, y), :, m * 128 : m * 128 + 128] = result[b * 16 : b * 16 + 16]

    def emit(zz):
        g = mixed[pl.ds(zz * 8, 8)].reshape(2, 64, 384)
        p = nt(g[0], w_cat[0]) + nt(g[1], w_cat[1])
        row = iota((8, 128), 0)
        for pair in range(2):
            both = []
            for yy in (2 * pair, 2 * pair + 1):
                both.append(p[yy * 16 : yy * 16 + 8, :128] + p[yy * 16 + 8 : yy * 16 + 16, 128:])
            even = both[0] + pltpu.roll(pltpu.roll(both[0], 64, 1), 4, 0)
            odd = pltpu.roll(both[1], 4, 0) + pltpu.roll(both[1], 64, 1)
            at = pl.ds(pl.multiple_of(zz * 16 + pair * 8, 8), 8)
            raw[at, :] = jnp.where(row < 4, even, odd)

    step = gather_over_torus(mixed, mix_send, mix_recv, (z, y), lambda t: None, emit)
    lax.fori_loop(1, HALF + 3, step, 0)

    result = raw[...].T
    final_out[...] = jnp.where(c == 0, result[32:64], result[:32]).astype(BF16)
    final[c] = jnp.where(c == 0, result[:32], result[32:64]).astype(BF16)
    final_copy = pltpu.make_async_remote_copy(
        src_ref=final_out,
        dst_ref=final.at[c],
        send_sem=pair_send.at[3],
        recv_sem=pair_recv.at[3],
        device_id=other,
        device_id_type=MESH,
    )
    final_copy.start()
    drain(tokens, tok_send, tok_recv.at[0], 126)
    drain(mixed, mix_send, mix_recv.at[0], 126)
    weights_copy.wait_send()
    wo_copy.wait_send()
    partial_copy.wait_send()
    pltpu.make_async_copy(state, carried_hbm, store_sem).wait()
    final_copy.wait()
    out_ref[...] = nt(jnp.concatenate([final[0], final[1]], axis=1), order[...]).astype(BF16)


def per_device(
    tokens,
    norm_gain,
    w_query,
    w_key,
    w_value,
    w_gate,
    w_output,
    decay_rate,
    state,
    prev_keys,
    prev_values,
    accepted,
    parents,
    seq_length,
):
    smem = pl.BlockSpec(memory_space=pltpu.SMEM)
    hbm = pl.BlockSpec(memory_space=pl.ANY)
    dma = pltpu.SemaphoreType.DMA
    out, carried = pl.pallas_call(
        kernel,
        out_shape=(
            jax.ShapeDtypeStruct((32, 512), BF16),
            jax.ShapeDtypeStruct((24, 128, 128), F32),
        ),
        in_specs=[smem] * 4 + [hbm] * 10,
        out_specs=(pl.BlockSpec(memory_space=pltpu.VMEM), hbm),
        scratch_shapes=[
            pltpu.VMEM((32, 512), BF16),
            pltpu.VMEM((1, 4096), F32),
            pltpu.VMEM((4, 24, 4096), BF16),
            pltpu.VMEM((32, 3072), BF16),
            pltpu.VMEM((24, 128, 128), F32),
            pltpu.VMEM((4, 3072), BF16),
            pltpu.VMEM((4, 3072), BF16),
            pltpu.VMEM((512, 512), BF16),
            pltpu.VMEM((128, 16, 512), BF16),
            pltpu.VMEM((2, 96, 2048), BF16),
            pltpu.VMEM((96, 2048), BF16),
            pltpu.VMEM((2, 200, 256), F32),
            pltpu.VMEM((200, 256), F32),
            pltpu.VMEM((256, 256), F32),
            pltpu.VMEM((SLOTS, 4, 256), BF16),
            pltpu.VMEM((SLOTS, 4, 256), BF16),
            pltpu.VMEM((8, 32, 256), F32),
            pltpu.VMEM((24, 128, 128), BF16),
            pltpu.VMEM((24, 8, 128), F32),
            pltpu.VMEM((128, 16, 384), BF16),
            pltpu.VMEM((32, 3072), BF16),
            pltpu.VMEM((2, 256, 384), BF16),
            pltpu.VMEM((256, 128), F32),
            pltpu.VMEM((32, 256), BF16),
            pltpu.VMEM((2, 32, 256), BF16),
            dma((10,)),
            dma,
            dma((4,)),
            dma((4,)),
            dma,
            dma((128,)),
            dma,
            dma,
            dma,
            dma((128,)),
        ],
        compiler_params=pltpu.CompilerParams(collective_id=0, has_side_effects=True),
    )(
        accepted,
        parents,
        seq_length,
        decay_rate,
        tokens.T,
        norm_gain.reshape(1, -1),
        w_query.T,
        w_key.T,
        w_value.T,
        w_gate.T,
        w_output.T,
        state[0],
        prev_keys[0],
        prev_values[0],
    )
    return out.T, carried[None]


def solution(mesh):
    torus = Mesh(
        mesh.devices.reshape(mesh.shape["dp"], 16, 4, mesh.shape["tp"]),
        ("dp", "kv_0", "kv_1", "tp"),
    )
    in_specs = (
        P("dp", KV_TP),
        P(),
        P(None, KV_TP),
        P(None, KV_TP),
        P(None, KV_TP),
        P(None, KV_TP),
        P(None, KV_TP),
        P(),
        P(DP_KV_TP, None, None, None),
        P(DP_KV_TP, None, None),
        P(DP_KV_TP, None, None),
        P(DP_KV_TP),
        P(DP_KV_TP, None),
        P(DP_KV_TP),
    )
    out_specs = (P("dp", KV_TP), P(DP_KV_TP, None, None, None))
    return jax.shard_map(
        per_device, mesh=torus, in_specs=in_specs, out_specs=out_specs, check_vma=False
    )
```

time: 266 us -> 103 us (0.39)
  blocking collectives: 103 us -> 0 us
  waiting for transfers between devices: 103 us -> 0 us
  Pallas kernels: 0 us -> 96.7 us
  starting transfers between devices: 25.8 us -> 0 us
  local copies, waits for them, and re-layouts: 15.9 us -> 4.08 us
  matrix products: 8.22 us -> 0 us
  other arithmetic: 6.18 us -> 0 us
    all_to_all x3 -> x0, blocking collectives: 103 us -> none  [from_everyone(): return lax.all_to_all(copies, axis, split_axis=0, concat_axis=0, tiled=True)]
    all_to_all x2 -> x0, waiting for transfers between devices: 103 us -> none  [the longest x1 91 us: from_everyone(): return lax.all_to_all(copies, axis, split_axis=0, concat_axis=0, tiled=True)]
    pallas_call x0 -> x1, Pallas kernels: none -> 96.7 us  [per_device(): pl.pallas_call(kernel, out_shape=(jax.ShapeDtypeStruct((32, 512), BF16),...]
    all_to_all x2 -> x0, starting transfers between devices: 25.8 us -> none  [the longest x1 19.3 us: from_everyone(): return lax.all_to_all(copies, axis, split_axis=0, concat_axis=0, tiled=True)]
    dot_general x9 -> x0, matrix products: 8.22 us -> none  [the longest x1 2.27 us: advance(): jnp.einsum('bphd,bphe->bhde', old_keys * weights[..., None], old_values,...]
    another operation x1 -> x0, local copies, waits for them, and re-layouts: 4.49 us -> none  [in_order(): pieces.reshape(*dims[:dim], dims[dim] * dims[dim + 1], *dims[dim + 2:])]
    broadcast_in_dim x4 -> x0, local copies, waits for them, and re-layouts: 4.3 us -> none  [from_everyone(): copies = jnp.broadcast_to(array, (lax.axis_size(axis), *array.shape))]
    transpose x1 -> x0, local copies, waits for them, and re-layouts: 3.5 us -> none  [whole_of(): pieces = jnp.swapaxes(from_everyone(initial, near), 0, 1)]
  transfers between devices with their start and end apart: 2 -> 0, of which waited for: 2 -> 0; matrix products, arithmetic and copies ran while one was open for 2% -> 0% of each run, Pallas kernels for 0% -> 0%
where the time goes in v1:
time: 103 us
  Pallas kernels  96.7 us (94%)
  local copies, waits for them, and re-layouts  4.08 us (4%)
  between operations  1.94 us (2%)
    pallas_call x1, Pallas kernels, per_device(): pl.pallas_call(kernel, out_shape=(jax.ShapeDtypeStruct((32, 512), BF16),...  96.7 us
    unnamed x2, local copies, waits for them, and re-layouts  4.08 us

profile of v1, /device:TPU:1, one launch (start us, length us, event | category | flops | bytes accessed | tf_op | source)
XLA Modules:
  0.0 102.8 jit_solution(2384359735109439128)
XLA Ops:
  1.9 96.7 %shard_map.149 = (bf16[32,512]{1,0:T(8,128)(2,1)}, f32[24,128,128]{2,1,0:T(8,128)}) custom-call(s32[1]{0:T(128)S(6)} %copy.18.accepted_ref, s32[1,4]{1,0:T(1,128)} %parents_ref.1, s32[1]{0:T(128)S(6)} %copy.19.length_ref, f32[24]{0:T(128)} %decay_ref.1, bf16[32,512]{1,0:T(8,128)(2,1)} %bitcast.19, f32[1,4096]{1,0:T(1,128)} %bitcast.23, ...), custom_call_target="tpu_custom_call" | custom-call | tf_op jit(solution)/shard_map/pallas_call | solution.py:595
  98.7 1.4 %copy.20 = bf16[512,32]{0,1:T(8,128)(2,1)} copy(bf16[512,32]{0,1:T(8,128)(2,1)} %bitcast.20) | data formatting | bytes 65536
  100.1 2.7 %copy.21 = f32[1,24,128,128]{3,2,1,0:T(8,128)} copy(f32[1,24,128,128]{3,2,1,0:T(8,128)} %bitcast.13) | data formatting | bytes 3145728

commit v2 on v1

--- a/solution.py
+++ b/solution.py
@@ -17,7 +17,6 @@
 
 NZ, NY = 16, 4
 SLOTS = NZ * NY
-HALF = NZ // 2
 
 
 def iota(shape, axis):
@@ -30,10 +29,6 @@
 
 def tn(a, b):
     return lax.dot_general(a, b, (((0,), (0,)), ((), ())), preferred_element_type=F32)
-
-
-def block_of(z, h, y):
-    return z * (2 * NY) + h * NY + y
 
 
 def sin_cos(angle):
@@ -55,15 +50,32 @@
     return sine, cosine
 
 
+STAGES = [(0, 0, 0.0)] + [
+    (d, side, at)
+    for d, at in ((1, 3.2), (2, 3.6), (4, 5.0), (3, 6.6), (5, 8.2), (6, 8.9), (7, 9.6))
+    for side in (1, -1)
+] + [(8, 1, 10.4)]
+
+
+def agenda():
+    events = []
+    for i, (_, _, at) in enumerate(STAGES):
+        near = max(at + 2.9, 2.9 + 0.9 * i)
+        events += [(at, 0, i), (near, 1, i), (near + 2.9, 2, i)]
+    return sorted(events)
+
+
 def gather_over_torus(buf, send_sem, recv_sem, place, between, compute):
-    z, y = place
-    z_up, z_down = lax.rem(z + 1, NZ), lax.rem(z + NZ - 1, NZ)
-    y_up, y_down = lax.rem(y + 1, NY), lax.rem(y + NY - 1, NY)
-    y_far = lax.rem(y + 2, NY)
-    up, down = {"kv_0": z_up}, {"kv_0": z_down}
-    right, left = {"kv_1": y_up}, {"kv_1": y_down}
-
-    def copy(block, device):
+    z, y, c = place
+
+    def at_z(d):
+        return lax.rem(z + d + 2 * NZ, NZ)
+
+    def at_y(d):
+        return lax.rem(y + d + 2 * NY, NY)
+
+    def copy(zz, ys, device):
+        block = zz * NY + ys
         return pltpu.make_async_remote_copy(
             src_ref=buf.at[block],
             dst_ref=buf.at[block],
@@ -73,116 +85,46 @@
             device_id_type=MESH,
         )
 
-    def send(block, device):
-        copy(block, device).start()
-
-    def arrive(block):
-        copy(block, up).wait_recv()
-
-    for h in (0, 1):
-        own = block_of(z, h, y)
-        send(own, up)
-        send(own, down)
-    for h in (0, 1):
-        own = block_of(z, h, y)
-        send(own, right)
-        send(own, left)
-
-    def along(k, h, ys, last_up, last_down, spread):
-        z_from_down = lax.rem(z - k + 2 * NZ, NZ)
-        z_from_up = lax.rem(z + k, NZ)
-
-        @pl.when((k >= 1) & (k <= last_up))
-        def _():
-            block = block_of(z_from_down, h, ys)
-            arrive(block)
-
-            @pl.when(k < last_up)
-            def _():
-                send(block, up)
-
-            if spread:
-                send(block, right)
-                send(block, left)
-
-        @pl.when((k >= 1) & (k <= last_down))
-        def _():
-            block = block_of(z_from_up, h, ys)
-            arrive(block)
-
-            @pl.when(k < last_down)
-            def _():
-                send(block, down)
-
-            if spread:
-                send(block, right)
-                send(block, left)
-
-    def relay(zz, h, ys):
-        block = block_of(zz, h, ys)
-        even = lax.rem(zz, 2) == 0
-        if ys is y_down:
-
-            @pl.when(even)
-            def _():
-                send(block, right)
-
-        elif ys is y_up:
-
-            @pl.when(jnp.logical_not(even))
-            def _():
-                send(block, left)
-
-    def across(k, ys):
-        along(k, 0, ys, HALF, HALF - 1, False)
-
-        @pl.when(k == 0)
-        def _():
-            block = block_of(z, 0, ys)
-            arrive(block)
-            send(block, up)
-            send(block, down)
-            relay(z, 0, ys)
-            arrive(block_of(z, 1, ys))
-            relay(z, 1, ys)
-
-        @pl.when((k >= 1) & (k <= HALF - 1))
-        def _():
-            zz = lax.rem(z - k + 2 * NZ, NZ)
-            arrive(block_of(zz, 1, ys))
-            relay(zz, 1, ys)
-
-        @pl.when((k >= 1) & (k <= HALF))
-        def _():
-            zz = lax.rem(z + k, NZ)
-            arrive(block_of(zz, 1, ys))
-            relay(zz, 1, ys)
-
-    def step(t, carry):
-        @pl.when(t <= HALF)
-        def _():
-            along(t, 0, y, HALF, HALF - 1, False)
-            along(t, 1, y, HALF - 1, HALF, True)
-
-        @pl.when(t <= HALF + 1)
-        def _():
-            across(t - 1, y_down)
-            across(t - 1, y_up)
-
-        @pl.when(t >= 2)
-        def _():
-            k = t - 2
-            across(k, y_far)
-            compute(lax.rem(z - k + 2 * NZ, NZ))
-
-            @pl.when((k >= 1) & (k <= HALF - 1))
-            def _():
-                compute(lax.rem(z + k, NZ))
-
-        between(t)
-        return carry
-
-    return step
+    def send(zz, ys, dz=0, dy=0):
+        copy(zz, ys, {"kv_0": at_z(dz)} if dz else {"kv_1": at_y(dy)}).start()
+
+    def arrive(zz, ys):
+        copy(zz, ys, {"kv_1": at_y(1)}).wait_recv()
+
+    def run():
+        for _, kind, i in agenda():
+            d, side, _ = STAGES[i]
+            zz = at_z(-side * d)
+            if kind == 0:
+                if d == 0:
+                    for far in (4, -4, 2, -2, 1, -1):
+                        send(z, y, dz=far)
+                else:
+                    arrive(zz, y)
+                if d == 2:
+                    send(zz, y, dz=side)
+                if d == 4:
+                    for far in (3, 2, 1):
+                        send(zz, y, dz=side * far)
+
+                    @pl.when(c == (0 if side == 1 else 1))
+                    def _():
+                        send(zz, y, dz=side * 4)
+
+                send(zz, y, dy=1)
+                send(zz, y, dy=-1)
+            elif kind == 1:
+                turn = 1 if i % 2 else -1
+                for dy in (-turn, turn):
+                    arrive(zz, at_y(dy))
+                    if dy == -turn:
+                        send(zz, at_y(dy), dy=turn)
+            else:
+                arrive(zz, at_y(2))
+                compute(zz)
+            between(kind, i)
+
+    return run
 
 
 def drain(buf, send_sem, recv_sem, count):
@@ -197,10 +139,10 @@
 
 
 def kernel(
-    accepted_ref,
-    parents_ref,
-    length_ref,
-    decay_ref,
+    accepted_hbm,
+    parents_hbm,
+    length_hbm,
+    decay_hbm,
     tok_hbm,
     gain_hbm,
     wq_hbm,
@@ -213,6 +155,10 @@
     pv_hbm,
     out_ref,
     carried_hbm,
+    accepted_ref,
+    parents_ref,
+    length_ref,
+    decay_ref,
     tok,
     gain,
     w4,
@@ -263,17 +209,19 @@
         pltpu.make_async_copy(pk_hbm, pk, load_sem.at[7]),
         pltpu.make_async_copy(pv_hbm, pv, load_sem.at[8]),
         pltpu.make_async_copy(state_hbm, state, load_sem.at[9]),
+        pltpu.make_async_copy(accepted_hbm, accepted_ref, load_sem.at[10]),
+        pltpu.make_async_copy(parents_hbm, parents_ref, load_sem.at[11]),
+        pltpu.make_async_copy(length_hbm, length_ref, load_sem.at[12]),
+        pltpu.make_async_copy(decay_hbm, decay_ref, load_sem.at[13]),
     ]
     for load in loads:
         load.start()
     barrier = pltpu.get_barrier_semaphore()
-    for device in (
-        {"kv_0": lax.rem(z + 1, NZ)},
-        {"kv_0": lax.rem(z + NZ - 1, NZ)},
+    for device in [{"kv_0": lax.rem(z + d, NZ)} for d in (1, 2, 3, 4, 12, 13, 14, 15)] + [
         {"kv_1": lax.rem(y + 1, NY)},
         {"kv_1": lax.rem(y + NY - 1, NY)},
         other,
-    ):
+    ]:
         pl.semaphore_signal(barrier, inc=1, device_id=device, device_id_type=MESH)
 
     t = iota((512, 512), 0)
@@ -281,13 +229,12 @@
     order[...] = jnp.where(place == iota((512, 512), 1), 1.0, 0.0).astype(BF16)
     loads[0].wait()
     own = jnp.dot(tok[...], order[...], preferred_element_type=F32).astype(BF16)
-    tokens[block_of(z, 0, y)] = own[:16]
-    tokens[block_of(z, 1, y)] = own[16:]
+    tokens[slot] = own
     acc[...] = jnp.zeros_like(acc)
-    pl.semaphore_wait(barrier, 5)
+    pl.semaphore_wait(barrier, 11)
 
     def project(zz):
-        x = tokens[pl.ds(zz * 8, 8)].reshape(128, 512)
+        x = tokens[pl.ds(zz * NY, NY)].reshape(128, 512)
         w = weights[:, :, pl.ds(pl.multiple_of(zz * 128, 128), 128)].reshape(192, 128)
         r = jnp.dot(w, x, preferred_element_type=F32)
         xf = x.astype(F32)
@@ -297,46 +244,43 @@
             acc[half, :192] += r[:, lanes]
             acc[half, 192:] += squares[:, lanes]
 
-    def advance(t):
-        steps = accepted_ref[0].astype(F32)
-        g = t - 1
-
-        @pl.when(t == 1)
-        def _():
+    def advance(g):
+        steps = accepted_ref[0, 0].astype(F32)
+        lanes = slice(g * 384, g * 384 + 384)
+        keys = pk[:, lanes].astype(F32)
+        values = pv[:, lanes]
+        row = iota((4, 128), 0).astype(F32)
+        age = jnp.maximum(steps - 1.0 - row, 0.0)
+        for m in range(3):
+            h = g * 3 + m
+            r = jnp.broadcast_to(decay_ref[h], (8, 128))
+            decays[h] = r
+            weight = jnp.where(row < steps, jnp.exp(-r[:4] * age), 0.0)
+            part = slice(m * 128, m * 128 + 128)
+            keyed = keys[:, part] * weight
+            high = keyed.astype(BF16)
+            low = (keyed - high.astype(F32)).astype(BF16)
+            v = values[:, part]
+            added = tn(high, v) + tn(low, v)
+            kept = jnp.exp(-r[:1] * steps)
+            new = state[h] * kept + added
+            state[h] = new
+            carried_bf[m * 8 + (g % 2) * 4 + g // 2] = new.astype(BF16)
+
+    store = pltpu.make_async_copy(state, carried_hbm, store_sem)
+
+    def beside(kind, i):
+        if kind == 0 and i == 0:
             prepare_weights()
+        if kind == 1 and i == 0:
             for load in loads[6:]:
                 load.wait()
-            for h in range(24):
-                decays[h] = jnp.broadcast_to(decay_ref[h], (8, 128))
-
-        @pl.when((t >= 1) & (t <= 8))
-        def _():
-            lanes = pl.ds(pl.multiple_of(g * 384, 128), 384)
-            keys = pk[:, lanes].astype(F32)
-            values = pv[:, lanes]
-            row = iota((4, 128), 0).astype(F32)
-            for m in range(3):
-                h = g * 3 + m
-                r = decays[h]
-                age = jnp.maximum(steps - 1.0 - row, 0.0)
-                weight = jnp.where(row < steps, jnp.exp(-r[:4] * age), 0.0)
-                part = slice(m * 128, m * 128 + 128)
-                keyed = keys[:, part] * weight
-                high = keyed.astype(BF16)
-                low = (keyed - high.astype(F32)).astype(BF16)
-                v = values[:, part]
-                added = tn(high, v) + tn(low, v)
-                kept = jnp.exp(-r[:1] * steps)
-                new = state[h] * kept + added
-                state[h] = new
-                place = m * 8 + lax.rem(g, 2) * 4 + lax.div(g, 2)
-                carried_bf[place] = new.astype(BF16)
-
-        @pl.when(t == 9)
-        def _():
-            pltpu.make_async_copy(state, carried_hbm, store_sem).start()
-
-    step = gather_over_torus(tokens, tok_send, tok_recv, (z, y), advance, project)
+        if kind == 1 and i < 8:
+            advance(i)
+        if kind == 1 and i == 8:
+            store.start()
+
+    gather = gather_over_torus(tokens, tok_send, tok_recv, (z, y, c), beside, project)
     weights_copy = pltpu.make_async_remote_copy(
         src_ref=weights_out,
         dst_ref=weights.at[c],
@@ -357,8 +301,7 @@
     def prepare_weights():
         f = iota((256, 256), 0)
         yy, cc = lax.shift_right_logical(f, 6), lax.shift_right_logical(f, 5) & 1
-        hh, ii = lax.shift_right_logical(f, 4) & 1, f & 15
-        split = jnp.where(cc * 128 + hh * 64 + yy * 16 + ii == iota((256, 256), 1), 1.0, 0.0)
+        split = jnp.where(cc * 128 + yy * 32 + (f & 31) == iota((256, 256), 1), 1.0, 0.0)
         split = split.astype(BF16)
         for load in loads[1:6]:
             load.wait()
@@ -377,7 +320,7 @@
         weights_copy.start()
         weights_copy.wait_recv()
 
-    lax.fori_loop(1, HALF + 3, step, 0)
+    gather()
 
     partial_copy = pltpu.make_async_remote_copy(
         src_ref=acc.at[1 - c],
@@ -414,18 +357,28 @@
     lax.fori_loop(0, SLOTS // 2, pack, 0)
 
     def dispatch(i, carry):
-        target = lax.rem(slot + i, SLOTS)
-        pltpu.make_async_remote_copy(
-            src_ref=sent.at[target],
-            dst_ref=got.at[slot],
-            send_sem=a2a_send,
-            recv_sem=a2a_recv,
-            device_id={"kv_0": lax.div(target, NY), "kv_1": lax.rem(target, NY)},
-            device_id_type=MESH,
-        ).start()
+        odd = i & 1
+        zz = lax.rem(z + 8 + (1 - 2 * odd) * lax.shift_right_logical(i + 1, 1), NZ)
+        for dy in (2, 1, 3, 0):
+
+            def go(dy=dy):
+                yy = lax.rem(y + dy, NY)
+                pltpu.make_async_remote_copy(
+                    src_ref=sent.at[zz * NY + yy],
+                    dst_ref=got.at[slot],
+                    send_sem=a2a_send,
+                    recv_sem=a2a_recv,
+                    device_id={"kv_0": zz, "kv_1": yy},
+                    device_id_type=MESH,
+                ).start()
+
+            if dy:
+                go()
+            else:
+                pl.when(i < NZ - 1)(go)
         return carry
 
-    lax.fori_loop(1, SLOTS, dispatch, 0)
+    lax.fori_loop(0, NZ, dispatch, 0)
     got[slot] = sent[slot]
 
     parent = [parents_ref[0, i] for i in range(4)]
@@ -446,7 +399,7 @@
             result = jnp.where(p == i, values[i], result)
         return result
 
-    start = (length_ref[0] + accepted_ref[0]).astype(F32)
+    start = (length_ref[0, 0] + accepted_ref[0, 0]).astype(F32)
     lane = iota((8, 128), 1)
     freq = jnp.ones((8, 128), F32)
     for bit in range(6):
@@ -472,12 +425,11 @@
         near.append([linked[d] * jnp.exp(-rate * spacing[d]) for d in range(4)])
         carry_in.append(jnp.exp(-rate * (depths + 1.0)))
     wo_copy.wait_recv()
-    for b in range(2):
-        for jj in range(4):
-            lanes = slice((2 * jj + b) * 384, (2 * jj + b) * 384 + 384)
-            mine, theirs = wo[:, lanes], wo_in[:, lanes]
-            w_cat[b, jj * 64 : jj * 64 + 32] = jnp.where(c == 0, mine, theirs)
-            w_cat[b, jj * 64 + 32 : jj * 64 + 64] = jnp.where(c == 0, theirs, mine)
+    for jj in range(4):
+        lanes = slice(jj * 768, jj * 768 + 768)
+        mine, theirs = wo[:, lanes], wo_in[:, lanes]
+        w_cat[jj * 64 : jj * 64 + 32] = jnp.where(c == 0, mine, theirs)
+        w_cat[jj * 64 + 32 : jj * 64 + 64] = jnp.where(c == 0, theirs, mine)
 
     pltpu.make_async_remote_copy(
         src_ref=sent.at[pl.ds(0, SLOTS - 1)],
@@ -533,11 +485,11 @@
         result = (centred * lax.rsqrt(variance + EPS)) * (gate / (1.0 + jnp.exp(-gate)))
         result = result.astype(BF16)
         for b in range(2):
-            mixed[block_of(z, b, y), :, m * 128 : m * 128 + 128] = result[b * 16 : b * 16 + 16]
+            at = (b * 3 + m) * 128
+            mixed[slot, :, at : at + 128] = result[b * 16 : b * 16 + 16]
 
     def emit(zz):
-        g = mixed[pl.ds(zz * 8, 8)].reshape(2, 64, 384)
-        p = nt(g[0], w_cat[0]) + nt(g[1], w_cat[1])
+        p = nt(mixed[pl.ds(zz * NY, NY)].reshape(64, 768), w_cat[...])
         row = iota((8, 128), 0)
         for pair in range(2):
             both = []
@@ -548,8 +500,7 @@
             at = pl.ds(pl.multiple_of(zz * 16 + pair * 8, 8), 8)
             raw[at, :] = jnp.where(row < 4, even, odd)
 
-    step = gather_over_torus(mixed, mix_send, mix_recv, (z, y), lambda t: None, emit)
-    lax.fori_loop(1, HALF + 3, step, 0)
+    gather_over_torus(mixed, mix_send, mix_recv, (z, y, c), lambda kind, i: None, emit)()
 
     result = raw[...].T
     final_out[...] = jnp.where(c == 0, result[32:64], result[:32]).astype(BF16)
@@ -563,14 +514,32 @@
         device_id_type=MESH,
     )
     final_copy.start()
-    drain(tokens, tok_send, tok_recv.at[0], 126)
-    drain(mixed, mix_send, mix_recv.at[0], 126)
+    drain(tokens, tok_send, tok_recv.at[0], 63)
+    drain(mixed, mix_send, mix_recv.at[0], 63)
     weights_copy.wait_send()
     wo_copy.wait_send()
     partial_copy.wait_send()
-    pltpu.make_async_copy(state, carried_hbm, store_sem).wait()
+    store.wait()
     final_copy.wait()
     out_ref[...] = nt(jnp.concatenate([final[0], final[1]], axis=1), order[...]).astype(BF16)
+
+
+def hand_on(out_hbm, carried_hbm, out_to, carried_to, out, carried, load_sem, store_sem):
+    pieces = [(out_hbm, out, out_to)]
+    for i in range(6):
+        part = pl.ds(4 * i, 4)
+        pieces.append((carried_hbm.at[part], carried.at[part], carried_to.at[part]))
+    loads, stores = [], []
+    for i, (source, held, target) in enumerate(pieces):
+        loads.append(pltpu.make_async_copy(source, held, load_sem.at[i]))
+        stores.append(pltpu.make_async_copy(held, target, store_sem.at[i]))
+    for load in loads:
+        load.start()
+    for load, store in zip(loads, stores):
+        load.wait()
+        store.start()
+    for store in stores:
+        store.wait()
 
 
 def per_device(
@@ -589,7 +558,7 @@
     parents,
     seq_length,
 ):
-    smem = pl.BlockSpec(memory_space=pltpu.SMEM)
+    vmem = pl.BlockSpec(memory_space=pltpu.VMEM)
     hbm = pl.BlockSpec(memory_space=pl.ANY)
     dma = pltpu.SemaphoreType.DMA
     out, carried = pl.pallas_call(
@@ -598,9 +567,13 @@
             jax.ShapeDtypeStruct((32, 512), BF16),
             jax.ShapeDtypeStruct((24, 128, 128), F32),
         ),
-        in_specs=[smem] * 4 + [hbm] * 10,
-        out_specs=(pl.BlockSpec(memory_space=pltpu.VMEM), hbm),
+        in_specs=[hbm] * 14,
+        out_specs=(vmem, hbm),
         scratch_shapes=[
+            pltpu.SMEM((1, 1), jnp.int32),
+            pltpu.SMEM((1, 4), jnp.int32),
+            pltpu.SMEM((1, 1), jnp.int32),
+            pltpu.SMEM((24,), F32),
             pltpu.VMEM((32, 512), BF16),
             pltpu.VMEM((1, 4096), F32),
             pltpu.VMEM((4, 24, 4096), BF16),
@@ -609,7 +582,7 @@
             pltpu.VMEM((4, 3072), BF16),
             pltpu.VMEM((4, 3072), BF16),
             pltpu.VMEM((512, 512), BF16),
-            pltpu.VMEM((128, 16, 512), BF16),
+            pltpu.VMEM((SLOTS, 32, 512), BF16),
             pltpu.VMEM((2, 96, 2048), BF16),
             pltpu.VMEM((96, 2048), BF16),
             pltpu.VMEM((2, 200, 256), F32),
@@ -620,28 +593,28 @@
             pltpu.VMEM((8, 32, 256), F32),
             pltpu.VMEM((24, 128, 128), BF16),
             pltpu.VMEM((24, 8, 128), F32),
-            pltpu.VMEM((128, 16, 384), BF16),
+            pltpu.VMEM((SLOTS, 16, 768), BF16),
             pltpu.VMEM((32, 3072), BF16),
-            pltpu.VMEM((2, 256, 384), BF16),
+            pltpu.VMEM((256, 768), BF16),
             pltpu.VMEM((256, 128), F32),
             pltpu.VMEM((32, 256), BF16),
             pltpu.VMEM((2, 32, 256), BF16),
-            dma((10,)),
+            dma((14,)),
             dma,
             dma((4,)),
             dma((4,)),
             dma,
-            dma((128,)),
+            dma((SLOTS,)),
             dma,
             dma,
             dma,
-            dma((128,)),
+            dma((SLOTS,)),
         ],
         compiler_params=pltpu.CompilerParams(collective_id=0, has_side_effects=True),
     )(
-        accepted,
+        accepted[None],
         parents,
-        seq_length,
+        seq_length[None],
         decay_rate,
         tokens.T,
         norm_gain.reshape(1, -1),
@@ -654,6 +627,21 @@
         prev_keys[0],
         prev_values[0],
     )
+    out, carried = pl.pallas_call(
+        hand_on,
+        out_shape=(
+            jax.ShapeDtypeStruct((32, 512), BF16),
+            jax.ShapeDtypeStruct((24, 128, 128), F32),
+        ),
+        in_specs=[hbm, hbm],
+        out_specs=(hbm, hbm),
+        scratch_shapes=[
+            pltpu.VMEM((32, 512), BF16),
+            pltpu.VMEM((24, 128, 128), F32),
+            dma((7,)),
+            dma((7,)),
+        ],
+    )(out, carried)
     return out.T, carried[None]
 
 

time: 103 us -> 85.7 us (0.83)
  Pallas kernels: 96.7 us -> 83.6 us
  local copies, waits for them, and re-layouts: 4.08 us -> 0 us
    pallas_call x1, Pallas kernels: 96.7 us -> 81.4 us  [per_device(): pl.pallas_call(kernel, out_shape=(jax.ShapeDtypeStruct((32, 512), BF16),...]
    unnamed x2 -> x0, local copies, waits for them, and re-layouts: 4.08 us -> none
    pallas_call x0 -> x1, Pallas kernels: none -> 2.22 us  [per_device(): pl.pallas_call(hand_on, out_shape=(jax.ShapeDtypeStruct((32, 512), BF16),...]
where the time goes in v2:
time: 85.7 us; the launch traced here: 85.5 us
  Pallas kernels  83.6 us (98%)
  between operations  1.93 us (2%)
    pallas_call x1, Pallas kernels, per_device(): pl.pallas_call(kernel, out_shape=(jax.ShapeDtypeStruct((32, 512), BF16),...  81.4 us
    pallas_call x1, Pallas kernels, per_device(): pl.pallas_call(hand_on, out_shape=(jax.ShapeDtypeStruct((32, 512), BF16),...  2.22 us

profile of v2, /device:TPU:1, one launch (start us, length us, event | category | flops | bytes accessed | tf_op | source)
XLA Modules:
  0.0 85.5 jit_solution(17359872839565817259)
XLA Ops:
  1.9 81.4 %shard_map.149 = (bf16[32,512]{1,0:T(8,128)(2,1)}, f32[24,128,128]{2,1,0:T(8,128)}) custom-call(s32[1,1]{1,0:T(1,128)} %bitcast.14.accepted_hbm, s32[1,4]{1,0:T(1,128)} %parents_hbm.1, s32[1,1]{1,0:T(1,128)} %bitcast.15.length_hbm, f32[24]{0:T(128)} %decay_hbm.1, bf16[32,512]{1,0:T(8,128)(2,1)} %bitcast.22, f32[1,4096]{1,0:T(1,128)} %bitcast.25, ...), custom_call_target="tpu_custom_call" | custom-call | tf_op jit(solution)/shard_map/pallas_call | solution.py:564
  83.3 2.2 %shard_map.150 = (bf16[32,512]{1,0:T(8,128)(2,1)}, f32[24,128,128]{2,1,0:T(8,128)}) custom-call(bf16[32,512]{1,0:T(8,128)(2,1)} %get-tuple-element.6.out_hbm, f32[24,128,128]{2,1,0:T(8,128)} %get-tuple-element.7.carried_hbm), custom_call_target="tpu_custom_call" | custom-call | tf_op jit(solution)/shard_map/pallas_call | solution.py:630

commit v3 on v2

--- a/solution.py
+++ b/solution.py
@@ -50,81 +50,180 @@
     return sine, cosine
 
 
-STAGES = [(0, 0, 0.0)] + [
-    (d, side, at)
-    for d, at in ((1, 3.2), (2, 3.6), (4, 5.0), (3, 6.6), (5, 8.2), (6, 8.9), (7, 9.6))
-    for side in (1, -1)
-] + [(8, 1, 10.4)]
-
-
-def agenda():
-    events = []
-    for i, (_, _, at) in enumerate(STAGES):
-        near = max(at + 2.9, 2.9 + 0.9 * i)
-        events += [(at, 0, i), (near, 1, i), (near + 2.9, 2, i)]
-    return sorted(events)
-
-
-def gather_over_torus(buf, send_sem, recv_sem, place, between, compute):
-    z, y, c = place
-
-    def at_z(d):
-        return lax.rem(z + d + 2 * NZ, NZ)
-
-    def at_y(d):
-        return lax.rem(y + d + 2 * NY, NY)
-
-    def copy(zz, ys, device):
-        block = zz * NY + ys
+TOKEN_PLAN = (
+    (0, (16, 48, 1, 4, 3,)),
+    (1, (9, 61, 2,)),
+    (3, (59, 63,)),
+    (4, (8, 5, 7,)),
+    (16, (19, 28, 17,)),
+    (48, (40, 49, 52, 51,)),
+    (2, ()),
+    (61, (57, 62,)),
+    (5, (6,)),
+    (7, ()),
+    (63, (60,)),
+    (8, (12, 11,)),
+    (9, (10,)),
+    (59, (55, 58,)),
+    (19, (23, 18,)),
+    (17, (21,)),
+    (49, (37, 45,)),
+    (52, (53,)),
+    (51, (47, 50,)),
+    (62, ()),
+    (57, (56,)),
+    (6, ()),
+    (40, (43,)),
+    (60, ()),
+    (28, (24, 29, 31, 32,)),
+    (11, ()),
+    (12, (13,)),
+    (10, (14,)),
+    (55, ()),
+    (58, ()),
+    (23, (22, 20,)),
+    (18, (34,)),
+    (21, (25,)),
+    (53, (54,)),
+    (50, ()),
+    (45, (41, 44, 46,)),
+    (56, ()),
+    (47, ()),
+    (43, (39, 42,)),
+    (29, (33, 30,)),
+    (24, (27,)),
+    (31, (35,)),
+    (32, ()),
+    (13, ()),
+    (37, (36, 38,)),
+    (22, (26,)),
+    (14, (15,)),
+    (20, ()),
+    (54, ()),
+    (25, ()),
+    (44, ()),
+    (41, ()),
+    (46, ()),
+    (42, ()),
+    (39, ()),
+    (30, ()),
+    (33, ()),
+    (27, ()),
+    (36, ()),
+    (35, ()),
+    (38, ()),
+    (26, ()),
+    (15, ()),
+    (34, ()),
+)
+MIXED_PLAN = (
+    (0, (24, 52, 4, 16, 1, 3,)),
+    (1, (2,)),
+    (3, ()),
+    (4, (5, 60, 12, 7,)),
+    (52, (36, 53, 48, 55, 56,)),
+    (2, (62,)),
+    (16, (19, 20, 17,)),
+    (5, (6, 9,)),
+    (7, ()),
+    (24, (27, 25, 32,)),
+    (60, (61, 63,)),
+    (12, ()),
+    (53, (54,)),
+    (48, (44, 49,)),
+    (55, (47, 51,)),
+    (56, (57, 59,)),
+    (19, (15, 18,)),
+    (62, ()),
+    (17, (13,)),
+    (20, (23,)),
+    (6, (10,)),
+    (9, (8,)),
+    (27, (26, 31,)),
+    (25, (29, 21,)),
+    (36, (37, 40, 39,)),
+    (61, ()),
+    (63, ()),
+    (32, (33, 35,)),
+    (54, (42,)),
+    (44, (45,)),
+    (49, (41, 50,)),
+    (57, (58,)),
+    (51, ()),
+    (59, ()),
+    (15, (14,)),
+    (18, ()),
+    (13, ()),
+    (23, ()),
+    (47, (43, 46,)),
+    (8, ()),
+    (10, (11,)),
+    (26, (34, 22,)),
+    (31, (28,)),
+    (29, (30,)),
+    (37, (38,)),
+    (21, ()),
+    (39, ()),
+    (40, ()),
+    (33, ()),
+    (35, ()),
+    (45, ()),
+    (50, ()),
+    (58, ()),
+    (41, ()),
+    (14, ()),
+    (43, ()),
+    (46, ()),
+    (42, ()),
+    (11, ()),
+    (28, ()),
+    (22, ()),
+    (30, ()),
+    (38, ()),
+    (34, ()),
+)
+
+
+def step_of(a, b):
+    dz, dy = (b // NY - a // NY) % NZ, (b - a) % NY
+    return dz - NZ if dz > NZ // 2 else dz, -1 if dy == 3 else dy
+
+
+def steps_along_z():
+    return sorted({abs(step_of(a, b)[0]) for a, nexts in TOKEN_PLAN for b in nexts} - {0})
+
+
+def gather_over_torus(buf, send_sem, recv_sem, place, plan, between, compute):
+    z, y, way = place
+
+    devices = {}
+
+    def device(step):
+        if step not in devices:
+            dz, dy = step
+            devices[step] = {"kv_0": (z + way * dz) & (NZ - 1)} if dz else {"kv_1": (y + way * dy) & (NY - 1)}
+        return devices[step]
+
+    def copy(source, target, step):
         return pltpu.make_async_remote_copy(
-            src_ref=buf.at[block],
-            dst_ref=buf.at[block],
+            src_ref=buf.at[source],
+            dst_ref=buf.at[target],
             send_sem=send_sem,
-            recv_sem=recv_sem.at[block],
-            device_id=device,
+            recv_sem=recv_sem.at[target],
+            device_id=device(step),
             device_id_type=MESH,
         )
 
-    def send(zz, ys, dz=0, dy=0):
-        copy(zz, ys, {"kv_0": at_z(dz)} if dz else {"kv_1": at_y(dy)}).start()
-
-    def arrive(zz, ys):
-        copy(zz, ys, {"kv_1": at_y(1)}).wait_recv()
-
-    def run():
-        for _, kind, i in agenda():
-            d, side, _ = STAGES[i]
-            zz = at_z(-side * d)
-            if kind == 0:
-                if d == 0:
-                    for far in (4, -4, 2, -2, 1, -1):
-                        send(z, y, dz=far)
-                else:
-                    arrive(zz, y)
-                if d == 2:
-                    send(zz, y, dz=side)
-                if d == 4:
-                    for far in (3, 2, 1):
-                        send(zz, y, dz=side * far)
-
-                    @pl.when(c == (0 if side == 1 else 1))
-                    def _():
-                        send(zz, y, dz=side * 4)
-
-                send(zz, y, dy=1)
-                send(zz, y, dy=-1)
-            elif kind == 1:
-                turn = 1 if i % 2 else -1
-                for dy in (-turn, turn):
-                    arrive(zz, at_y(dy))
-                    if dy == -turn:
-                        send(zz, at_y(dy), dy=turn)
-            else:
-                arrive(zz, at_y(2))
-                compute(zz)
-            between(kind, i)
-
-    return run
+    seen = [0] * NZ
+    for i, (at, nexts) in enumerate(plan):
+        if at:
+            copy(at, at, (0, 1)).wait_recv()
+        for further in nexts:
+            copy(at, further, step_of(at, further)).start()
+        between(i)
+        seen[at // NY] += 1
+        if seen[at // NY] == NY:
+            compute(at // NY)
 
 
 def drain(buf, send_sem, recv_sem, count):
@@ -198,6 +297,15 @@
     z, y, c = lax.axis_index("kv_0"), lax.axis_index("kv_1"), lax.axis_index("tp")
     slot = z * NY + y
     other = {"tp": 1 - c}
+    barrier = pltpu.get_barrier_semaphore()
+    along_z = [d for step in steps_along_z() for d in sorted({step, NZ - step})]
+    for device in [{"kv_0": lax.rem(z + d, NZ)} for d in along_z] + [
+        {"kv_1": lax.rem(y + 1, NY)},
+        {"kv_1": lax.rem(y + NY - 1, NY)},
+        other,
+    ]:
+        pl.semaphore_signal(barrier, inc=1, device_id=device, device_id_type=MESH)
+
     loads = [
         pltpu.make_async_copy(tok_hbm, tok, load_sem.at[0]),
         pltpu.make_async_copy(gain_hbm, gain, load_sem.at[1]),
@@ -210,31 +318,27 @@
         pltpu.make_async_copy(pv_hbm, pv, load_sem.at[8]),
         pltpu.make_async_copy(state_hbm, state, load_sem.at[9]),
         pltpu.make_async_copy(accepted_hbm, accepted_ref, load_sem.at[10]),
+        pltpu.make_async_copy(length_hbm, length_ref, load_sem.at[12]),
         pltpu.make_async_copy(parents_hbm, parents_ref, load_sem.at[11]),
-        pltpu.make_async_copy(length_hbm, length_ref, load_sem.at[12]),
         pltpu.make_async_copy(decay_hbm, decay_ref, load_sem.at[13]),
     ]
-    for load in loads:
-        load.start()
-    barrier = pltpu.get_barrier_semaphore()
-    for device in [{"kv_0": lax.rem(z + d, NZ)} for d in (1, 2, 3, 4, 12, 13, 14, 15)] + [
-        {"kv_1": lax.rem(y + 1, NY)},
-        {"kv_1": lax.rem(y + NY - 1, NY)},
-        other,
-    ]:
-        pl.semaphore_signal(barrier, inc=1, device_id=device, device_id_type=MESH)
-
+    loads[0].start()
     t = iota((512, 512), 0)
-    place = (lax.shift_right_logical(t, 2) & 1) * 256 + lax.shift_right_logical(t, 3) * 4 + (t & 3)
-    order[...] = jnp.where(place == iota((512, 512), 1), 1.0, 0.0).astype(BF16)
+    moved = (lax.shift_right_logical(t, 2) & 1) * 256 + lax.shift_right_logical(t, 3) * 4 + (t & 3)
+    order[...] = jnp.where(moved == iota((512, 512), 1), 1.0, 0.0).astype(BF16)
     loads[0].wait()
     own = jnp.dot(tok[...], order[...], preferred_element_type=F32).astype(BF16)
-    tokens[slot] = own
-    acc[...] = jnp.zeros_like(acc)
-    pl.semaphore_wait(barrier, 11)
-
-    def project(zz):
-        x = tokens[pl.ds(zz * NY, NY)].reshape(128, 512)
+    tokens[0] = own
+    pl.semaphore_wait(barrier, len(along_z) + 3)
+
+    waited = []
+
+    def project(dz):
+        if not waited:
+            weights_copy.wait_recv()
+            waited.append(True)
+        zz = (z - way * dz) & (NZ - 1)
+        x = tokens[dz * NY : dz * NY + NY].reshape(128, 512)
         w = weights[:, :, pl.ds(pl.multiple_of(zz * 128, 128), 128)].reshape(192, 128)
         r = jnp.dot(w, x, preferred_element_type=F32)
         xf = x.astype(F32)
@@ -245,7 +349,7 @@
             acc[half, 192:] += squares[:, lanes]
 
     def advance(g):
-        steps = accepted_ref[0, 0].astype(F32)
+        steps = accepted_ref[0].astype(F32)
         lanes = slice(g * 384, g * 384 + 384)
         keys = pk[:, lanes].astype(F32)
         values = pv[:, lanes]
@@ -269,18 +373,22 @@
 
     store = pltpu.make_async_copy(state, carried_hbm, store_sem)
 
-    def beside(kind, i):
-        if kind == 0 and i == 0:
+    def beside(i):
+        if i == 0:
+            for load in loads[1:]:
+                load.start()
+            acc[...] = jnp.zeros_like(acc)
             prepare_weights()
-        if kind == 1 and i == 0:
+        if i == 4:
             for load in loads[6:]:
                 load.wait()
-        if kind == 1 and i < 8:
-            advance(i)
-        if kind == 1 and i == 8:
+        if i >= 6 and i % 3 == 0 and i < 30:
+            advance(i // 3 - 2)
+        if i == 30:
             store.start()
 
-    gather = gather_over_torus(tokens, tok_send, tok_recv, (z, y, c), beside, project)
+    way = 1 - 2 * c
+    place = (z, y, way)
     weights_copy = pltpu.make_async_remote_copy(
         src_ref=weights_out,
         dst_ref=weights.at[c],
@@ -301,6 +409,7 @@
     def prepare_weights():
         f = iota((256, 256), 0)
         yy, cc = lax.shift_right_logical(f, 6), lax.shift_right_logical(f, 5) & 1
+        yy = ((1 - 2 * cc) * (y - yy)) & (NY - 1)
         split = jnp.where(cc * 128 + yy * 32 + (f & 31) == iota((256, 256), 1), 1.0, 0.0)
         split = split.astype(BF16)
         for load in loads[1:6]:
@@ -318,9 +427,8 @@
 
         lax.fori_loop(0, NZ, chunk, 0)
         weights_copy.start()
-        weights_copy.wait_recv()
-
-    gather()
+
+    gather_over_torus(tokens, tok_send, tok_recv, place, TOKEN_PLAN, beside, project)
 
     partial_copy = pltpu.make_async_remote_copy(
         src_ref=acc.at[1 - c],
@@ -399,7 +507,7 @@
             result = jnp.where(p == i, values[i], result)
         return result
 
-    start = (length_ref[0, 0] + accepted_ref[0, 0]).astype(F32)
+    start = (length_ref[0] + accepted_ref[0]).astype(F32)
     lane = iota((8, 128), 1)
     freq = jnp.ones((8, 128), F32)
     for bit in range(6):
@@ -424,6 +532,12 @@
             rate = jnp.where(group == at, jnp.concatenate([decays[3 * g + m]] * 4, axis=0), rate)
         near.append([linked[d] * jnp.exp(-rate * spacing[d]) for d in range(4)])
         carry_in.append(jnp.exp(-rate * (depths + 1.0)))
+    t = iota((512, 512), 0)
+    core = lax.shift_right_logical(t, 2) & 1
+    dz = ((1 - 2 * core) * (z - lax.shift_right_logical(t, 5))) & (NZ - 1)
+    dy = ((1 - 2 * core) * (y - lax.shift_right_logical(t, 3))) & (NY - 1)
+    moved = core * 256 + dz * 16 + dy * 4 + (t & 3)
+    order[...] = jnp.where(moved == iota((512, 512), 1), 1.0, 0.0).astype(BF16)
     wo_copy.wait_recv()
     for jj in range(4):
         lanes = slice(jj * 768, jj * 768 + 768)
@@ -486,10 +600,10 @@
         result = result.astype(BF16)
         for b in range(2):
             at = (b * 3 + m) * 128
-            mixed[slot, :, at : at + 128] = result[b * 16 : b * 16 + 16]
-
-    def emit(zz):
-        p = nt(mixed[pl.ds(zz * NY, NY)].reshape(64, 768), w_cat[...])
+            mixed[0, :, at : at + 128] = result[b * 16 : b * 16 + 16]
+
+    def emit(dz):
+        p = nt(mixed[dz * NY : dz * NY + NY].reshape(64, 768), w_cat[...])
         row = iota((8, 128), 0)
         for pair in range(2):
             both = []
@@ -497,10 +611,10 @@
                 both.append(p[yy * 16 : yy * 16 + 8, :128] + p[yy * 16 + 8 : yy * 16 + 16, 128:])
             even = both[0] + pltpu.roll(pltpu.roll(both[0], 64, 1), 4, 0)
             odd = pltpu.roll(both[1], 4, 0) + pltpu.roll(both[1], 64, 1)
-            at = pl.ds(pl.multiple_of(zz * 16 + pair * 8, 8), 8)
-            raw[at, :] = jnp.where(row < 4, even, odd)
-
-    gather_over_torus(mixed, mix_send, mix_recv, (z, y, c), lambda kind, i: None, emit)()
+            at = dz * 16 + pair * 8
+            raw[at : at + 8, :] = jnp.where(row < 4, even, odd)
+
+    gather_over_torus(mixed, mix_send, mix_recv, place, MIXED_PLAN, lambda i: None, emit)
 
     result = raw[...].T
     final_out[...] = jnp.where(c == 0, result[32:64], result[:32]).astype(BF16)
@@ -570,9 +684,9 @@
         in_specs=[hbm] * 14,
         out_specs=(vmem, hbm),
         scratch_shapes=[
-            pltpu.SMEM((1, 1), jnp.int32),
+            pltpu.SMEM((1,), jnp.int32),
             pltpu.SMEM((1, 4), jnp.int32),
-            pltpu.SMEM((1, 1), jnp.int32),
+            pltpu.SMEM((1,), jnp.int32),
             pltpu.SMEM((24,), F32),
             pltpu.VMEM((32, 512), BF16),
             pltpu.VMEM((1, 4096), F32),
@@ -612,9 +726,9 @@
         ],
         compiler_params=pltpu.CompilerParams(collective_id=0, has_side_effects=True),
     )(
-        accepted[None],
+        accepted,
         parents,
-        seq_length[None],
+        seq_length,
         decay_rate,
         tokens.T,
         norm_gain.reshape(1, -1),

time: 85.7 us -> 77.4 us (0.903)
  Pallas kernels: 83.6 us -> 75.2 us
    pallas_call x1, Pallas kernels: 81.4 us -> 73 us  [per_device(): pl.pallas_call(kernel, out_shape=(jax.ShapeDtypeStruct((32, 512), BF16),...]
where the time goes in v3:
time: 77.4 us; the launch traced here: 77.1 us
  Pallas kernels  75.2 us (97%)
  between operations  1.93 us (2%)
    pallas_call x1, Pallas kernels, per_device(): pl.pallas_call(kernel, out_shape=(jax.ShapeDtypeStruct((32, 512), BF16),...  73 us
    pallas_call x1, Pallas kernels, per_device(): pl.pallas_call(hand_on, out_shape=(jax.ShapeDtypeStruct((32, 512), BF16),...  2.22 us

profile of v3, /device:TPU:1, one launch (start us, length us, event | category | flops | bytes accessed | tf_op | source)
XLA Modules:
  0.0 77.1 jit_solution(916537379510943597)
XLA Ops:
  1.9 73.0 %shard_map.149 = (bf16[32,512]{1,0:T(8,128)(2,1)}, f32[24,128,128]{2,1,0:T(8,128)}) custom-call(s32[1]{0:T(128)S(6)} %copy.16.accepted_hbm, s32[1,4]{1,0:T(1,128)} %parents_hbm.1, s32[1]{0:T(128)S(6)} %copy.17.length_hbm, f32[24]{0:T(128)} %decay_hbm.1, bf16[32,512]{1,0:T(8,128)(2,1)} %bitcast.18, f32[1,4096]{1,0:T(1,128)} %bitcast.21, ...), custom_call_target="tpu_custom_call" | custom-call | tf_op jit(solution)/shard_map/pallas_call | solution.py:678
  74.9 2.2 %shard_map.150 = (bf16[32,512]{1,0:T(8,128)(2,1)}, f32[24,128,128]{2,1,0:T(8,128)}) custom-call(bf16[32,512]{1,0:T(8,128)(2,1)} %get-tuple-element.6.out_hbm, f32[24,128,128]{2,1,0:T(8,128)} %get-tuple-element.7.carried_hbm), custom_call_target="tpu_custom_call" | custom-call | tf_op jit(solution)/shard_map/pallas_call | solution.py:744

commit v4 on v2

--- a/solution.py
+++ b/solution.py
@@ -50,81 +50,320 @@
     return sine, cosine
 
 
-STAGES = [(0, 0, 0.0)] + [
-    (d, side, at)
-    for d, at in ((1, 3.2), (2, 3.6), (4, 5.0), (3, 6.6), (5, 8.2), (6, 8.9), (7, 9.6))
-    for side in (1, -1)
-] + [(8, 1, 10.4)]
-
-
-def agenda():
-    events = []
-    for i, (_, _, at) in enumerate(STAGES):
-        near = max(at + 2.9, 2.9 + 0.9 * i)
-        events += [(at, 0, i), (near, 1, i), (near + 2.9, 2, i)]
-    return sorted(events)
-
-
-def gather_over_torus(buf, send_sem, recv_sem, place, between, compute):
+TOKEN_PLAN = (
+    (
+        (0, (48, 16, 1, 3,)),
+        (1, (9, 53, 5, 2, 61,)),
+        (3, (63,)),
+        (48, (51, 40, 49, 44,)),
+        (16, (28, 19, 17, 20,)),
+        (2, (62,)),
+        (5, (6, 4,)),
+        (61, ()),
+        (63, (60,)),
+        (9, (8, 13,)),
+        (53, (57, 52, 54,)),
+        (51, (50,)),
+        (49, (37,)),
+        (19, (18, 23,)),
+        (17, (21,)),
+        (44, (47, 45,)),
+        (20, ()),
+        (40, (36, 41, 43,)),
+        (4, ()),
+        (6, (10, 7,)),
+        (60, (56,)),
+        (28, (31, 24, 32, 29,)),
+        (62, ()),
+        (8, (11,)),
+        (13, (12, 14,)),
+        (52, (55,)),
+        (54, ()),
+        (57, (58,)),
+        (50, (34,)),
+        (18, (26,)),
+        (21, (25,)),
+        (45, ()),
+        (47, (46,)),
+        (23, (27, 22,)),
+        (36, (39,)),
+        (41, (42,)),
+        (37, (33, 38,)),
+        (7, ()),
+        (43, ()),
+        (10, ()),
+        (56, (59,)),
+        (31, (35, 30,)),
+        (24, ()),
+        (11, (15,)),
+        (32, ()),
+        (29, ()),
+        (12, ()),
+        (55, ()),
+        (14, ()),
+        (58, ()),
+        (46, ()),
+        (25, ()),
+        (22, ()),
+        (27, ()),
+        (39, ()),
+        (26, ()),
+        (42, ()),
+        (33, ()),
+        (59, ()),
+        (35, ()),
+        (38, ()),
+        (30, ()),
+        (34, ()),
+        (15, ()),
+    ),
+    (
+        (0, (12, 52, 3, 1,)),
+        (3, (63, 2,)),
+        (1, (5, 61,)),
+        (12, (15, 16, 20, 13,)),
+        (52, (44, 53, 56, 55,)),
+        (2, ()),
+        (63, (62, 60,)),
+        (61, ()),
+        (5, (4, 6,)),
+        (15, (23, 11, 14,)),
+        (13, ()),
+        (16, (17, 19,)),
+        (55, (51,)),
+        (53, (49, 54,)),
+        (62, (58,)),
+        (60, ()),
+        (56, (57,)),
+        (4, (7,)),
+        (6, ()),
+        (20, (24,)),
+        (44, (36, 45,)),
+        (14, ()),
+        (17, (18, 21,)),
+        (11, (8,)),
+        (19, ()),
+        (54, ()),
+        (51, ()),
+        (23, (27, 35, 22,)),
+        (49, (48, 50,)),
+        (7, ()),
+        (57, ()),
+        (24, (28,)),
+        (45, (46,)),
+        (58, (59,)),
+        (18, (10,)),
+        (21, ()),
+        (8, (9,)),
+        (36, (40, 37, 39,)),
+        (50, ()),
+        (22, ()),
+        (27, (26,)),
+        (48, ()),
+        (46, (42, 47,)),
+        (28, (29,)),
+        (59, ()),
+        (9, ()),
+        (40, (41,)),
+        (39, (43,)),
+        (10, ()),
+        (37, (33, 38,)),
+        (26, (30, 25,)),
+        (35, (31, 32, 34,)),
+        (42, ()),
+        (47, ()),
+        (29, ()),
+        (41, ()),
+        (43, ()),
+        (33, ()),
+        (38, ()),
+        (25, ()),
+        (30, ()),
+        (31, ()),
+        (32, ()),
+        (34, ()),
+    ),
+)
+MIXED_PLAN = (
+    (
+        (0, (20, 40, 3, 1, 8, 52,)),
+        (3, (63, 15, 2,)),
+        (1, (49, 5, 61,)),
+        (8, (16, 9, 11,)),
+        (52, (55, 53,)),
+        (20, (32, 21, 24, 23,)),
+        (2, (62,)),
+        (63, (59, 60,)),
+        (5, (4, 6,)),
+        (61, ()),
+        (40, (36, 41, 44,)),
+        (9, (10,)),
+        (11, ()),
+        (15, (14, 12,)),
+        (53, (54,)),
+        (16, (19, 17,)),
+        (55, (51, 47,)),
+        (21, (22,)),
+        (23, ()),
+        (49, (45,)),
+        (24, (28, 25, 27,)),
+        (60, ()),
+        (62, (50,)),
+        (4, (7,)),
+        (6, ()),
+        (59, (56, 58,)),
+        (41, (42, 37,)),
+        (44, ()),
+        (36, (39,)),
+        (32, (35, 33,)),
+        (10, ()),
+        (12, ()),
+        (14, (13,)),
+        (19, (18,)),
+        (54, ()),
+        (51, (48,)),
+        (17, ()),
+        (22, (30,)),
+        (25, (29,)),
+        (27, (26,)),
+        (7, ()),
+        (28, (31,)),
+        (45, (46,)),
+        (56, (57,)),
+        (58, ()),
+        (39, (38,)),
+        (47, ()),
+        (42, (43,)),
+        (35, (34,)),
+        (37, ()),
+        (33, ()),
+        (13, ()),
+        (18, ()),
+        (50, ()),
+        (26, ()),
+        (48, ()),
+        (29, ()),
+        (31, ()),
+        (46, ()),
+        (57, ()),
+        (30, ()),
+        (38, ()),
+        (43, ()),
+        (34, ()),
+    ),
+    (
+        (0, (16, 48, 3, 1,)),
+        (3, (11, 63,)),
+        (1, (2,)),
+        (16, (24, 19, 17,)),
+        (48, (44, 51, 52,)),
+        (2, (58,)),
+        (63, (60, 59, 62,)),
+        (11, (7, 10,)),
+        (19, (18,)),
+        (44, (45, 47,)),
+        (17, (13,)),
+        (51, (43,)),
+        (60, (56,)),
+        (52, (53,)),
+        (62, ()),
+        (59, ()),
+        (24, (32, 8, 20, 25, 28, 27,)),
+        (58, (57,)),
+        (10, (14, 6,)),
+        (7, (4,)),
+        (18, (22,)),
+        (45, (41, 49,)),
+        (13, (29,)),
+        (47, ()),
+        (53, (54,)),
+        (56, ()),
+        (57, ()),
+        (25, (26,)),
+        (28, ()),
+        (27, ()),
+        (20, (21,)),
+        (14, (30, 15,)),
+        (6, ()),
+        (4, (5,)),
+        (32, (35, 36, 33,)),
+        (43, (42, 39, 40,)),
+        (22, (34, 23,)),
+        (49, ()),
+        (41, (37,)),
+        (54, (50, 55,)),
+        (26, ()),
+        (21, ()),
+        (36, ()),
+        (35, (31,)),
+        (15, ()),
+        (42, (38, 46,)),
+        (39, ()),
+        (5, (61, 9,)),
+        (8, (12,)),
+        (33, ()),
+        (29, ()),
+        (37, ()),
+        (40, ()),
+        (50, ()),
+        (23, ()),
+        (55, ()),
+        (34, ()),
+        (31, ()),
+        (38, ()),
+        (30, ()),
+        (46, ()),
+        (9, ()),
+        (12, ()),
+        (61, ()),
+    ),
+)
+
+
+def step_of(a, b):
+    dz, dy = (b // NY - a // NY) % NZ, (b - a) % NY
+    return dz - NZ if dz > NZ // 2 else dz, -1 if dy == 3 else dy
+
+
+def steps_along_z():
+    rows = TOKEN_PLAN[0] + TOKEN_PLAN[1]
+    return sorted({abs(step_of(a, b)[0]) for a, nexts in rows for b in nexts} - {0})
+
+
+def gather_over_torus(buf, send_sem, recv_sem, place, plans, first, compute):
     z, y, c = place
 
-    def at_z(d):
-        return lax.rem(z + d + 2 * NZ, NZ)
-
-    def at_y(d):
-        return lax.rem(y + d + 2 * NY, NY)
-
-    def copy(zz, ys, device):
-        block = zz * NY + ys
+    def copy(source, target, step):
+        dz, dy = step
+        device = {"kv_0": (z + dz) & (NZ - 1)} if dz else {"kv_1": (y + dy) & (NY - 1)}
         return pltpu.make_async_remote_copy(
-            src_ref=buf.at[block],
-            dst_ref=buf.at[block],
+            src_ref=buf.at[source],
+            dst_ref=buf.at[target],
             send_sem=send_sem,
-            recv_sem=recv_sem.at[block],
+            recv_sem=recv_sem.at[target],
             device_id=device,
             device_id_type=MESH,
         )
 
-    def send(zz, ys, dz=0, dy=0):
-        copy(zz, ys, {"kv_0": at_z(dz)} if dz else {"kv_1": at_y(dy)}).start()
-
-    def arrive(zz, ys):
-        copy(zz, ys, {"kv_1": at_y(1)}).wait_recv()
-
-    def run():
-        for _, kind, i in agenda():
-            d, side, _ = STAGES[i]
-            zz = at_z(-side * d)
-            if kind == 0:
-                if d == 0:
-                    for far in (4, -4, 2, -2, 1, -1):
-                        send(z, y, dz=far)
-                else:
-                    arrive(zz, y)
-                if d == 2:
-                    send(zz, y, dz=side)
-                if d == 4:
-                    for far in (3, 2, 1):
-                        send(zz, y, dz=side * far)
-
-                    @pl.when(c == (0 if side == 1 else 1))
-                    def _():
-                        send(zz, y, dz=side * 4)
-
-                send(zz, y, dy=1)
-                send(zz, y, dy=-1)
-            elif kind == 1:
-                turn = 1 if i % 2 else -1
-                for dy in (-turn, turn):
-                    arrive(zz, at_y(dy))
-                    if dy == -turn:
-                        send(zz, at_y(dy), dy=turn)
-            else:
-                arrive(zz, at_y(2))
-                compute(zz)
-            between(kind, i)
-
-    return run
+    def forward(at, nexts):
+        for further in nexts:
+            copy(at, further, step_of(at, further)).start()
+
+    def rest(plan):
+        seen = [0] * NZ
+        seen[0] = 1
+        for at, nexts in plan[1:]:
+            copy(at, at, (0, 1)).wait_recv()
+            forward(at, nexts)
+            seen[at // NY] += 1
+            if seen[at // NY] == NY:
+                compute(at // NY)
+
+    for core, plan in enumerate(plans):
+        pl.when(c == core)(functools.partial(forward, *plan[0]))
+    first()
+    for core, plan in enumerate(plans):
+        pl.when(c == core)(functools.partial(rest, plan))
 
 
 def drain(buf, send_sem, recv_sem, count):
@@ -198,6 +437,15 @@
     z, y, c = lax.axis_index("kv_0"), lax.axis_index("kv_1"), lax.axis_index("tp")
     slot = z * NY + y
     other = {"tp": 1 - c}
+    barrier = pltpu.get_barrier_semaphore()
+    along_z = [d for step in steps_along_z() for d in sorted({step, NZ - step})]
+    for device in [{"kv_0": lax.rem(z + d, NZ)} for d in along_z] + [
+        {"kv_1": lax.rem(y + 1, NY)},
+        {"kv_1": lax.rem(y + NY - 1, NY)},
+        other,
+    ]:
+        pl.semaphore_signal(barrier, inc=1, device_id=device, device_id_type=MESH)
+
     loads = [
         pltpu.make_async_copy(tok_hbm, tok, load_sem.at[0]),
         pltpu.make_async_copy(gain_hbm, gain, load_sem.at[1]),
@@ -210,31 +458,23 @@
         pltpu.make_async_copy(pv_hbm, pv, load_sem.at[8]),
         pltpu.make_async_copy(state_hbm, state, load_sem.at[9]),
         pltpu.make_async_copy(accepted_hbm, accepted_ref, load_sem.at[10]),
+        pltpu.make_async_copy(length_hbm, length_ref, load_sem.at[12]),
         pltpu.make_async_copy(parents_hbm, parents_ref, load_sem.at[11]),
-        pltpu.make_async_copy(length_hbm, length_ref, load_sem.at[12]),
         pltpu.make_async_copy(decay_hbm, decay_ref, load_sem.at[13]),
     ]
     for load in loads:
         load.start()
-    barrier = pltpu.get_barrier_semaphore()
-    for device in [{"kv_0": lax.rem(z + d, NZ)} for d in (1, 2, 3, 4, 12, 13, 14, 15)] + [
-        {"kv_1": lax.rem(y + 1, NY)},
-        {"kv_1": lax.rem(y + NY - 1, NY)},
-        other,
-    ]:
-        pl.semaphore_signal(barrier, inc=1, device_id=device, device_id_type=MESH)
-
     t = iota((512, 512), 0)
-    place = (lax.shift_right_logical(t, 2) & 1) * 256 + lax.shift_right_logical(t, 3) * 4 + (t & 3)
-    order[...] = jnp.where(place == iota((512, 512), 1), 1.0, 0.0).astype(BF16)
+    moved = (lax.shift_right_logical(t, 2) & 1) * 256 + lax.shift_right_logical(t, 3) * 4 + (t & 3)
+    order[...] = jnp.where(moved == iota((512, 512), 1), 1.0, 0.0).astype(BF16)
     loads[0].wait()
     own = jnp.dot(tok[...], order[...], preferred_element_type=F32).astype(BF16)
-    tokens[slot] = own
-    acc[...] = jnp.zeros_like(acc)
-    pl.semaphore_wait(barrier, 11)
-
-    def project(zz):
-        x = tokens[pl.ds(zz * NY, NY)].reshape(128, 512)
+    tokens[0] = own
+    pl.semaphore_wait(barrier, len(along_z) + 3)
+
+    def project(dz):
+        zz = (z - dz) & (NZ - 1)
+        x = tokens[dz * NY : dz * NY + NY].reshape(128, 512)
         w = weights[:, :, pl.ds(pl.multiple_of(zz * 128, 128), 128)].reshape(192, 128)
         r = jnp.dot(w, x, preferred_element_type=F32)
         xf = x.astype(F32)
@@ -245,7 +485,7 @@
             acc[half, 192:] += squares[:, lanes]
 
     def advance(g):
-        steps = accepted_ref[0, 0].astype(F32)
+        steps = accepted_ref[0].astype(F32)
         lanes = slice(g * 384, g * 384 + 384)
         keys = pk[:, lanes].astype(F32)
         values = pv[:, lanes]
@@ -269,18 +509,12 @@
 
     store = pltpu.make_async_copy(state, carried_hbm, store_sem)
 
-    def beside(kind, i):
-        if kind == 0 and i == 0:
-            prepare_weights()
-        if kind == 1 and i == 0:
-            for load in loads[6:]:
-                load.wait()
-        if kind == 1 and i < 8:
-            advance(i)
-        if kind == 1 and i == 8:
-            store.start()
-
-    gather = gather_over_torus(tokens, tok_send, tok_recv, (z, y, c), beside, project)
+    def beside():
+        acc[...] = jnp.zeros_like(acc)
+        prepare_weights()
+        weights_copy.wait_recv()
+
+    place = (z, y, c)
     weights_copy = pltpu.make_async_remote_copy(
         src_ref=weights_out,
         dst_ref=weights.at[c],
@@ -301,6 +535,7 @@
     def prepare_weights():
         f = iota((256, 256), 0)
         yy, cc = lax.shift_right_logical(f, 6), lax.shift_right_logical(f, 5) & 1
+        yy = (y - yy) & (NY - 1)
         split = jnp.where(cc * 128 + yy * 32 + (f & 31) == iota((256, 256), 1), 1.0, 0.0)
         split = split.astype(BF16)
         for load in loads[1:6]:
@@ -318,9 +553,8 @@
 
         lax.fori_loop(0, NZ, chunk, 0)
         weights_copy.start()
-        weights_copy.wait_recv()
-
-    gather()
+
+    gather_over_torus(tokens, tok_send, tok_recv, place, TOKEN_PLAN, beside, project)
 
     partial_copy = pltpu.make_async_remote_copy(
         src_ref=acc.at[1 - c],
@@ -331,6 +565,7 @@
         device_id_type=MESH,
     )
     partial_copy.start()
+    loads[6].wait()
     wo_copy.start()
     partial_copy.wait_recv()
     total = acc[c] + acc_in[...]
@@ -381,6 +616,11 @@
     lax.fori_loop(0, NZ, dispatch, 0)
     got[slot] = sent[slot]
 
+    for load in loads[7:]:
+        load.wait()
+    for g in range(8):
+        advance(g)
+    store.start()
     parent = [parents_ref[0, i] for i in range(4)]
     one, zero = jnp.float32(1.0), jnp.float32(0.0)
     anc = [[one if i == k else zero for k in range(4)] for i in range(4)]
@@ -399,7 +639,7 @@
             result = jnp.where(p == i, values[i], result)
         return result
 
-    start = (length_ref[0, 0] + accepted_ref[0, 0]).astype(F32)
+    start = (length_ref[0] + accepted_ref[0]).astype(F32)
     lane = iota((8, 128), 1)
     freq = jnp.ones((8, 128), F32)
     for bit in range(6):
@@ -424,6 +664,11 @@
             rate = jnp.where(group == at, jnp.concatenate([decays[3 * g + m]] * 4, axis=0), rate)
         near.append([linked[d] * jnp.exp(-rate * spacing[d]) for d in range(4)])
         carry_in.append(jnp.exp(-rate * (depths + 1.0)))
+    t = iota((512, 512), 0)
+    dz = (z - lax.shift_right_logical(t, 5)) & (NZ - 1)
+    dy = (y - lax.shift_right_logical(t, 3)) & (NY - 1)
+    moved = (lax.shift_right_logical(t, 2) & 1) * 256 + dz * 16 + dy * 4 + (t & 3)
+    order[...] = jnp.where(moved == iota((512, 512), 1), 1.0, 0.0).astype(BF16)
     wo_copy.wait_recv()
     for jj in range(4):
         lanes = slice(jj * 768, jj * 768 + 768)
@@ -486,10 +731,10 @@
         result = result.astype(BF16)
         for b in range(2):
             at = (b * 3 + m) * 128
-            mixed[slot, :, at : at + 128] = result[b * 16 : b * 16 + 16]
-
-    def emit(zz):
-        p = nt(mixed[pl.ds(zz * NY, NY)].reshape(64, 768), w_cat[...])
+            mixed[0, :, at : at + 128] = result[b * 16 : b * 16 + 16]
+
+    def emit(dz):
+        p = nt(mixed[dz * NY : dz * NY + NY].reshape(64, 768), w_cat[...])
         row = iota((8, 128), 0)
         for pair in range(2):
             both = []
@@ -497,23 +742,24 @@
                 both.append(p[yy * 16 : yy * 16 + 8, :128] + p[yy * 16 + 8 : yy * 16 + 16, 128:])
             even = both[0] + pltpu.roll(pltpu.roll(both[0], 64, 1), 4, 0)
             odd = pltpu.roll(both[1], 4, 0) + pltpu.roll(both[1], 64, 1)
-            at = pl.ds(pl.multiple_of(zz * 16 + pair * 8, 8), 8)
-            raw[at, :] = jnp.where(row < 4, even, odd)
-
-    gather_over_torus(mixed, mix_send, mix_recv, (z, y, c), lambda kind, i: None, emit)()
+            at = dz * 16 + pair * 8
+            raw[at : at + 8, :] = jnp.where(row < 4, even, odd)
+
+    gather_over_torus(mixed, mix_send, mix_recv, place, MIXED_PLAN, lambda: None, emit)
 
     result = raw[...].T
     final_out[...] = jnp.where(c == 0, result[32:64], result[:32]).astype(BF16)
-    final[c] = jnp.where(c == 0, result[:32], result[32:64]).astype(BF16)
     final_copy = pltpu.make_async_remote_copy(
         src_ref=final_out,
-        dst_ref=final.at[c],
+        dst_ref=final,
         send_sem=pair_send.at[3],
         recv_sem=pair_recv.at[3],
         device_id=other,
         device_id_type=MESH,
     )
     final_copy.start()
+    mine = jnp.where(c == 0, result[:32], result[32:64]).astype(BF16)
+    mine = nt(mine, order[:, pl.ds(pl.multiple_of(c * 256, 256), 256)])
     drain(tokens, tok_send, tok_recv.at[0], 63)
     drain(mixed, mix_send, mix_recv.at[0], 63)
     weights_copy.wait_send()
@@ -521,7 +767,8 @@
     partial_copy.wait_send()
     store.wait()
     final_copy.wait()
-    out_ref[...] = nt(jnp.concatenate([final[0], final[1]], axis=1), order[...]).astype(BF16)
+    theirs = nt(final[...], order[:, pl.ds(pl.multiple_of((1 - c) * 256, 256), 256)])
+    out_ref[...] = (mine + theirs).astype(BF16)
 
 
 def hand_on(out_hbm, carried_hbm, out_to, carried_to, out, carried, load_sem, store_sem):
@@ -570,9 +817,9 @@
         in_specs=[hbm] * 14,
         out_specs=(vmem, hbm),
         scratch_shapes=[
-            pltpu.SMEM((1, 1), jnp.int32),
+            pltpu.SMEM((1,), jnp.int32),
             pltpu.SMEM((1, 4), jnp.int32),
-            pltpu.SMEM((1, 1), jnp.int32),
+            pltpu.SMEM((1,), jnp.int32),
             pltpu.SMEM((24,), F32),
             pltpu.VMEM((32, 512), BF16),
             pltpu.VMEM((1, 4096), F32),
@@ -598,7 +845,7 @@
             pltpu.VMEM((256, 768), BF16),
             pltpu.VMEM((256, 128), F32),
             pltpu.VMEM((32, 256), BF16),
-            pltpu.VMEM((2, 32, 256), BF16),
+            pltpu.VMEM((32, 256), BF16),
             dma((14,)),
             dma,
             dma((4,)),
@@ -612,9 +859,9 @@
         ],
         compiler_params=pltpu.CompilerParams(collective_id=0, has_side_effects=True),
     )(
-        accepted[None],
+        accepted,
         parents,
-        seq_length[None],
+        seq_length,
         decay_rate,
         tokens.T,
         norm_gain.reshape(1, -1),

time: 85.7 us -> 76.8 us (0.90)
  Pallas kernels: 83.6 us -> 74.7 us
    pallas_call x1, Pallas kernels: 81.4 us -> 72.4 us  [per_device(): pl.pallas_call(kernel, out_shape=(jax.ShapeDtypeStruct((32, 512), BF16),...]
where the time goes in v4:
time: 76.8 us; the launch traced here: 76.6 us
  Pallas kernels  74.7 us (97%)
  between operations  1.93 us (3%)
    pallas_call x1, Pallas kernels, per_device(): pl.pallas_call(kernel, out_shape=(jax.ShapeDtypeStruct((32, 512), BF16),...  72.4 us
    pallas_call x1, Pallas kernels, per_device(): pl.pallas_call(hand_on, out_shape=(jax.ShapeDtypeStruct((32, 512), BF16),...  2.22 us

profile of v4, /device:TPU:1, one launch (start us, length us, event | category | flops | bytes accessed | tf_op | source)
XLA Modules:
  0.0 76.6 jit_solution(3312625343457986874)
XLA Ops:
  1.9 72.4 %shard_map.149 = (bf16[32,512]{1,0:T(8,128)(2,1)}, f32[24,128,128]{2,1,0:T(8,128)}) custom-call(s32[1]{0:T(128)S(6)} %copy.16.accepted_hbm, s32[1,4]{1,0:T(1,128)} %parents_hbm.1, s32[1]{0:T(128)S(6)} %copy.17.length_hbm, f32[24]{0:T(128)} %decay_hbm.1, bf16[32,512]{1,0:T(8,128)(2,1)} %bitcast.18, f32[1,4096]{1,0:T(1,128)} %bitcast.21, ...), custom_call_target="tpu_custom_call" | custom-call | tf_op jit(solution)/shard_map/pallas_call | solution.py:811
  74.4 2.2 %shard_map.150 = (bf16[32,512]{1,0:T(8,128)(2,1)}, f32[24,128,128]{2,1,0:T(8,128)}) custom-call(bf16[32,512]{1,0:T(8,128)(2,1)} %get-tuple-element.6.out_hbm, f32[24,128,128]{2,1,0:T(8,128)} %get-tuple-element.7.carried_hbm), custom_call_target="tpu_custom_call" | custom-call | tf_op jit(solution)/shard_map/pallas_call | solution.py:877

commit v5 on v4

--- a/solution.py
+++ b/solution.py
@@ -59,43 +59,43 @@
         (16, (28, 19, 17, 20,)),
         (2, (62,)),
         (5, (6, 4,)),
-        (61, ()),
         (63, (60,)),
         (9, (8, 13,)),
+        (61, ()),
         (53, (57, 52, 54,)),
         (51, (50,)),
         (49, (37,)),
         (19, (18, 23,)),
         (17, (21,)),
         (44, (47, 45,)),
+        (40, (36, 41, 43,)),
+        (6, (10, 7,)),
         (20, ()),
-        (40, (36, 41, 43,)),
-        (4, ()),
-        (6, (10, 7,)),
         (60, (56,)),
         (28, (31, 24, 32, 29,)),
-        (62, ()),
         (8, (11,)),
+        (4, ()),
         (13, (12, 14,)),
         (52, (55,)),
-        (54, ()),
         (57, (58,)),
         (50, (34,)),
+        (62, ()),
         (18, (26,)),
         (21, (25,)),
-        (45, ()),
+        (54, ()),
         (47, (46,)),
         (23, (27, 22,)),
         (36, (39,)),
         (41, (42,)),
         (37, (33, 38,)),
+        (45, ()),
+        (56, (59,)),
+        (31, (35, 30,)),
+        (11, (15,)),
         (7, ()),
         (43, ()),
         (10, ()),
-        (56, (59,)),
-        (31, (35, 30,)),
         (24, ()),
-        (11, (15,)),
         (32, ()),
         (29, ()),
         (12, ()),
@@ -123,53 +123,53 @@
         (1, (5, 61,)),
         (12, (15, 16, 20, 13,)),
         (52, (44, 53, 56, 55,)),
+        (63, (62, 60,)),
+        (5, (4, 6,)),
         (2, ()),
-        (63, (62, 60,)),
+        (15, (23, 11, 14,)),
+        (16, (17, 19,)),
         (61, ()),
-        (5, (4, 6,)),
-        (15, (23, 11, 14,)),
-        (13, ()),
-        (16, (17, 19,)),
         (55, (51,)),
         (53, (49, 54,)),
         (62, (58,)),
-        (60, ()),
         (56, (57,)),
+        (13, ()),
         (4, (7,)),
-        (6, ()),
         (20, (24,)),
         (44, (36, 45,)),
+        (60, ()),
+        (17, (18, 21,)),
+        (6, ()),
+        (11, (8,)),
+        (23, (27, 35, 22,)),
         (14, ()),
-        (17, (18, 21,)),
-        (11, (8,)),
+        (49, (48, 50,)),
         (19, ()),
         (54, ()),
-        (51, ()),
-        (23, (27, 35, 22,)),
-        (49, (48, 50,)),
-        (7, ()),
-        (57, ()),
         (24, (28,)),
         (45, (46,)),
         (58, (59,)),
+        (51, ()),
+        (7, ()),
+        (57, ()),
         (18, (10,)),
-        (21, ()),
         (8, (9,)),
         (36, (40, 37, 39,)),
+        (27, (26,)),
+        (21, ()),
+        (46, (42, 47,)),
         (50, ()),
         (22, ()),
-        (27, (26,)),
+        (28, (29,)),
         (48, ()),
-        (46, (42, 47,)),
-        (28, (29,)),
-        (59, ()),
-        (9, ()),
         (40, (41,)),
         (39, (43,)),
-        (10, ()),
+        (59, ()),
         (37, (33, 38,)),
         (26, (30, 25,)),
         (35, (31, 32, 34,)),
+        (9, ()),
+        (10, ()),
         (42, ()),
         (47, ()),
         (29, ()),
@@ -186,136 +186,136 @@
 )
 MIXED_PLAN = (
     (
-        (0, (20, 40, 3, 1, 8, 52,)),
-        (3, (63, 15, 2,)),
-        (1, (49, 5, 61,)),
-        (8, (16, 9, 11,)),
-        (52, (55, 53,)),
-        (20, (32, 21, 24, 23,)),
+        (0, (48, 16, 1, 3,)),
+        (1, (9, 53, 5, 2, 61,)),
+        (3, (63,)),
+        (48, (51, 40, 49, 44,)),
+        (16, (28, 19, 17, 20,)),
         (2, (62,)),
-        (63, (59, 60,)),
-        (5, (4, 6,)),
+        (5, (6, 4,)),
+        (63, (60,)),
+        (9, (8, 13,)),
         (61, ()),
-        (40, (36, 41, 44,)),
-        (9, (10,)),
-        (11, ()),
-        (15, (14, 12,)),
-        (53, (54,)),
-        (16, (19, 17,)),
-        (55, (51, 47,)),
-        (21, (22,)),
-        (23, ()),
-        (49, (45,)),
-        (24, (28, 25, 27,)),
-        (60, ()),
-        (62, (50,)),
-        (4, (7,)),
-        (6, ()),
-        (59, (56, 58,)),
-        (41, (42, 37,)),
-        (44, ()),
+        (53, (57, 52, 54,)),
+        (51, (50,)),
+        (49, (37,)),
+        (44, (47, 45,)),
+        (19, (18, 23,)),
+        (17, (21,)),
+        (40, (36, 41, 43,)),
+        (6, (10, 7,)),
+        (20, ()),
+        (60, (56,)),
+        (28, (31, 24, 32, 29,)),
+        (8, (11,)),
+        (13, (12, 14,)),
+        (4, ()),
+        (62, ()),
+        (57, (58,)),
+        (52, (55,)),
+        (50, (34,)),
+        (47, (46,)),
+        (21, (25,)),
+        (18, (26,)),
+        (23, (27, 22,)),
+        (54, ()),
+        (41, (42,)),
         (36, (39,)),
-        (32, (35, 33,)),
+        (45, ()),
+        (37, (33, 38,)),
+        (56, (59,)),
+        (31, (35, 30,)),
+        (43, ()),
+        (11, (15,)),
         (10, ()),
+        (7, ()),
+        (24, ()),
+        (29, ()),
+        (32, ()),
+        (14, ()),
         (12, ()),
-        (14, (13,)),
-        (19, (18,)),
-        (54, ()),
-        (51, (48,)),
-        (17, ()),
-        (22, (30,)),
-        (25, (29,)),
-        (27, (26,)),
-        (7, ()),
-        (28, (31,)),
-        (45, (46,)),
-        (56, (57,)),
         (58, ()),
-        (39, (38,)),
-        (47, ()),
-        (42, (43,)),
-        (35, (34,)),
-        (37, ()),
+        (55, ()),
+        (25, ()),
+        (46, ()),
+        (22, ()),
+        (27, ()),
+        (42, ()),
+        (39, ()),
+        (26, ()),
+        (38, ()),
         (33, ()),
-        (13, ()),
-        (18, ()),
-        (50, ()),
-        (26, ()),
-        (48, ()),
-        (29, ()),
-        (31, ()),
-        (46, ()),
-        (57, ()),
+        (59, ()),
+        (35, ()),
+        (34, ()),
         (30, ()),
-        (38, ()),
-        (43, ()),
-        (34, ()),
+        (15, ()),
     ),
     (
-        (0, (16, 48, 3, 1,)),
-        (3, (11, 63,)),
-        (1, (2,)),
-        (16, (24, 19, 17,)),
-        (48, (44, 51, 52,)),
-        (2, (58,)),
-        (63, (60, 59, 62,)),
-        (11, (7, 10,)),
-        (19, (18,)),
-        (44, (45, 47,)),
-        (17, (13,)),
-        (51, (43,)),
-        (60, (56,)),
-        (52, (53,)),
-        (62, ()),
+        (0, (12, 52, 3, 1,)),
+        (3, (63, 2,)),
+        (1, (5, 61,)),
+        (12, (15, 16, 20, 13,)),
+        (52, (44, 53, 56, 55,)),
+        (63, (62, 60,)),
+        (5, (4, 6,)),
+        (2, ()),
+        (15, (23, 11, 14,)),
+        (16, (17, 19,)),
+        (61, ()),
+        (55, (51,)),
+        (53, (49, 54,)),
+        (56, (57,)),
+        (62, (58,)),
+        (44, (36, 45,)),
+        (20, (24,)),
+        (13, ()),
+        (4, (7,)),
+        (60, ()),
+        (11, (8,)),
+        (17, (18, 21,)),
+        (6, ()),
+        (49, (48, 50,)),
+        (23, (27, 35, 22,)),
+        (14, ()),
+        (24, (28,)),
+        (58, (59,)),
+        (19, ()),
+        (45, (46,)),
+        (54, ()),
+        (51, ()),
+        (57, ()),
+        (36, (40, 37, 39,)),
+        (7, ()),
+        (8, (9,)),
+        (18, (10,)),
+        (27, (26,)),
+        (21, ()),
+        (28, (29,)),
+        (46, (42, 47,)),
+        (50, ()),
+        (48, ()),
+        (37, (33, 38,)),
+        (39, (43,)),
+        (40, (41,)),
+        (22, ()),
         (59, ()),
-        (24, (32, 8, 20, 25, 28, 27,)),
-        (58, (57,)),
-        (10, (14, 6,)),
-        (7, (4,)),
-        (18, (22,)),
-        (45, (41, 49,)),
-        (13, (29,)),
+        (35, (31, 32, 34,)),
+        (26, (30, 25,)),
+        (9, ()),
+        (10, ()),
+        (29, ()),
+        (42, ()),
         (47, ()),
-        (53, (54,)),
-        (56, ()),
-        (57, ()),
-        (25, (26,)),
-        (28, ()),
-        (27, ()),
-        (20, (21,)),
-        (14, (30, 15,)),
-        (6, ()),
-        (4, (5,)),
-        (32, (35, 36, 33,)),
-        (43, (42, 39, 40,)),
-        (22, (34, 23,)),
-        (49, ()),
-        (41, (37,)),
-        (54, (50, 55,)),
-        (26, ()),
-        (21, ()),
-        (36, ()),
-        (35, (31,)),
-        (15, ()),
-        (42, (38, 46,)),
-        (39, ()),
-        (5, (61, 9,)),
-        (8, (12,)),
         (33, ()),
-        (29, ()),
-        (37, ()),
-        (40, ()),
-        (50, ()),
-        (23, ()),
-        (55, ()),
+        (43, ()),
+        (38, ()),
+        (41, ()),
         (34, ()),
+        (32, ()),
         (31, ()),
-        (38, ()),
         (30, ()),
-        (46, ()),
-        (9, ()),
-        (12, ()),
-        (61, ()),
+        (25, ()),
     ),
 )
 

time: 76.8 us -> 75.9 us (0.988)
  Pallas kernels: 74.7 us -> 73.8 us
    pallas_call x1, Pallas kernels: 72.4 us -> 71.5 us  [per_device(): pl.pallas_call(kernel, out_shape=(jax.ShapeDtypeStruct((32, 512), BF16),...]
where the time goes in v5:
time: 75.9 us; the launch traced here: 75.7 us
  Pallas kernels  73.8 us (97%)
  between operations  1.93 us (3%)
    pallas_call x1, Pallas kernels, per_device(): pl.pallas_call(kernel, out_shape=(jax.ShapeDtypeStruct((32, 512), BF16),...  71.5 us
    pallas_call x1, Pallas kernels, per_device(): pl.pallas_call(hand_on, out_shape=(jax.ShapeDtypeStruct((32, 512), BF16),...  2.22 us

profile of v5, /device:TPU:1, one launch (start us, length us, event | category | flops | bytes accessed | tf_op | source)
XLA Modules:
  0.0 75.7 jit_solution(15324749292301331190)
XLA Ops:
  1.9 71.5 %shard_map.149 = (bf16[32,512]{1,0:T(8,128)(2,1)}, f32[24,128,128]{2,1,0:T(8,128)}) custom-call(s32[1]{0:T(128)S(6)} %copy.16.accepted_hbm, s32[1,4]{1,0:T(1,128)} %parents_hbm.1, s32[1]{0:T(128)S(6)} %copy.17.length_hbm, f32[24]{0:T(128)} %decay_hbm.1, bf16[32,512]{1,0:T(8,128)(2,1)} %bitcast.18, f32[1,4096]{1,0:T(1,128)} %bitcast.21, ...), custom_call_target="tpu_custom_call" | custom-call | tf_op jit(solution)/shard_map/pallas_call | solution.py:811
  73.5 2.2 %shard_map.150 = (bf16[32,512]{1,0:T(8,128)(2,1)}, f32[24,128,128]{2,1,0:T(8,128)}) custom-call(bf16[32,512]{1,0:T(8,128)(2,1)} %get-tuple-element.6.out_hbm, f32[24,128,128]{2,1,0:T(8,128)} %get-tuple-element.7.carried_hbm), custom_call_target="tpu_custom_call" | custom-call | tf_op jit(solution)/shard_map/pallas_call | solution.py:877

commit v6 on v5

--- a/solution.py
+++ b/solution.py
@@ -566,8 +566,8 @@
     )
     partial_copy.start()
     loads[6].wait()
+    partial_copy.wait_recv()
     wo_copy.start()
-    partial_copy.wait_recv()
     total = acc[c] + acc_in[...]
     mean = jnp.sum(total[192:], axis=0, keepdims=True) * (1.0 / 4096.0)
     total = total[:192] * lax.rsqrt(mean + EPS)

time: 75.9 us -> 76.2 us (level)
  no operation moved by 1% of the time
where the time goes in v6:
time: 76.2 us; the launch traced here: 76 us
  Pallas kernels  74.1 us (97%)
  between operations  1.93 us (3%)
    pallas_call x1, Pallas kernels, per_device(): pl.pallas_call(kernel, out_shape=(jax.ShapeDtypeStruct((32, 512), BF16),...  71.8 us
    pallas_call x1, Pallas kernels, per_device(): pl.pallas_call(hand_on, out_shape=(jax.ShapeDtypeStruct((32, 512), BF16),...  2.22 us

profile of v6, /device:TPU:1, one launch (start us, length us, event | category | flops | bytes accessed | tf_op | source)
XLA Modules:
  0.0 76.0 jit_solution(13715010867868034217)
XLA Ops:
  1.9 71.8 %shard_map.149 = (bf16[32,512]{1,0:T(8,128)(2,1)}, f32[24,128,128]{2,1,0:T(8,128)}) custom-call(s32[1]{0:T(128)S(6)} %copy.16.accepted_hbm, s32[1,4]{1,0:T(1,128)} %parents_hbm.1, s32[1]{0:T(128)S(6)} %copy.17.length_hbm, f32[24]{0:T(128)} %decay_hbm.1, bf16[32,512]{1,0:T(8,128)(2,1)} %bitcast.18, f32[1,4096]{1,0:T(1,128)} %bitcast.21, ...), custom_call_target="tpu_custom_call" | custom-call | tf_op jit(solution)/shard_map/pallas_call | solution.py:811
  73.8 2.2 %shard_map.150 = (bf16[32,512]{1,0:T(8,128)(2,1)}, f32[24,128,128]{2,1,0:T(8,128)}) custom-call(bf16[32,512]{1,0:T(8,128)(2,1)} %get-tuple-element.6.out_hbm, f32[24,128,128]{2,1,0:T(8,128)} %get-tuple-element.7.carried_hbm), custom_call_target="tpu_custom_call" | custom-call | tf_op jit(solution)/shard_map/pallas_call | solution.py:877
